TPU v7x, 256 devices: a whole 4x4x8 slice. The times are simulated.
256 devices in a mesh: dp: 4 (over y), kv: 32 (over z, x), tp: 2 (over core).
Axes of the slice: x: 4, y: 4, z: 8, core: 2. Of those that a mesh axis runs over, the one named last changes fastest.
Arguments:
- tokens: bfloat16 [256, 4, 2048], P('dp', None, 'kv'), may hold values from -420 to 420
- input_norm_gain: bfloat16 [2048], replicated, may hold values from 0.099609375 to 1.8984375
- head_input_weight: bfloat16 [2048, 3072], P('kv', 'tp'), may hold values from -0.125 to 0.125
- output_gate_weight: bfloat16 [2048, 3072], P('kv', 'tp'), may hold values from -0.125 to 0.125
- state_maps_weight: bfloat16 [2048, 2, 1024], P('kv', None, 'tp'), may hold values from -0.125 to 0.125
- step_size_weight: bfloat16 [2048, 48], replicated, may hold values from -0.125 to 0.125
- step_size_bias: float32 [48], replicated, may hold values from -4 to -1
- head_decay_speed: float32 [48], replicated, may hold values from 0.3 to 8
- proposal_decay_total: float32 [256, 4, 48], P(('dp', 'kv'), None, 'tp'), may hold values from -0.7 to 0
- head_input_kernel: bfloat16 [4, 3072], replicated, may hold values from -3 to 3
- state_maps_kernel: bfloat16 [4, 2, 1024], replicated, may hold values from -3 to 3
- head_direct_gain: float32 [48], replicated, may hold values from 0.5 to 1.5
- grouped_norm_gain: bfloat16 [3072], replicated, may hold values from 0.099609375 to 1.8984375
- output_weight: bfloat16 [3072, 2048], P('tp', 'kv'), may hold values from -0.109375 to 0.109375
- prior_state_value: float32 [256, 48, 64, 128], P(('dp', 'kv'), 'tp'), may hold values from -2.4 to 2.4
- previous_head_input: bfloat16 [256, 4, 3072], P(('dp', 'kv'), None, 'tp'), may hold values from -2.390625 to 2.390625
- previous_input_maps: bfloat16 [256, 4, 1024], P(('dp', 'kv'), None, 'tp'), may hold values from -5 to 5
- previous_log_decays: float32 [256, 4, 48], P(('dp', 'kv'), None, 'tp'), may hold values from -1.5 to -0.05
- prior_heads_window: bfloat16 [256, 7, 3072], P(('dp', 'kv'), None, 'tp'), may hold values from -6 to 6
- prior_maps_window: bfloat16 [256, 7, 2, 1024], P(('dp', 'kv'), None, None, 'tp'), may hold values from -6 to 6
- accepted: int32 [256], P(('dp', 'kv')), may hold values from 1 to 4
Outputs:
- mixed: bfloat16 [256, 4, 2048], P('dp', None, 'kv')
- accepted_state: float32 [256, 48, 64, 128], P(('dp', 'kv'), 'tp')
- current_head_input: bfloat16 [256, 4, 3072], P(('dp', 'kv'), None, 'tp')
- current_input_maps: bfloat16 [256, 4, 1024], P(('dp', 'kv'), None, 'tp')
- current_log_decays: float32 [256, 4, 48], P(('dp', 'kv'), None, 'tp')
- current_heads_window: bfloat16 [256, 7, 3072], P(('dp', 'kv'), None, 'tp')
- current_maps_window: bfloat16 [256, 7, 2, 1024], P(('dp', 'kv'), None, None, 'tp')
All inputs are finite; a program needn't handle non-finite values.
Results may differ from a plain program's by a relative error of at most 0.029.
Values may be sent and summed in bfloat16 or wider, within the bound.
A program may use at most 64 MiB of HBM per device.

v0:
```python
import jax
import jax.numpy as jnp
from jax import lax
from jax.sharding import PartitionSpec as P

D = 2048
HEAD_DIM = 64
STATE = 128
CONV = 4


eps = 1e-06


def sent_to_all(array, axis):
    devices = lax.axis_size(axis)
    return lax.all_to_all(
        jnp.broadcast_to(array[None], (devices, *array.shape)), axis, 0, 0, tiled=True
    )


def taken_together(array, axis):
    everything = sent_to_all(array, axis)
    return jnp.sum(everything, axis=0)


def cut_along(array, dim, devices):
    before, after = (array.shape[:dim], array.shape[dim + 1 :])
    return jnp.moveaxis(array.reshape(*before, devices, -1, *after), dim, 0)


def summed_on_arrival(array, axis, dim):
    parts = cut_along(array, dim, lax.axis_size(axis))
    arrived = lax.all_to_all(parts, axis, split_axis=0, concat_axis=0, tiled=True)
    return arrived.astype(jnp.float32).sum(axis=0)


def shortened(array):

    def short(part):
        return part.astype(jnp.bfloat16) if part.dtype == jnp.float32 else part

    return jax.tree.map(short, array)


def joined_along(parts, dim):
    parts = jnp.moveaxis(parts, 0, dim)
    lengths = parts.shape
    return parts.reshape(*lengths[:dim], lengths[dim] * lengths[dim + 1], *lengths[dim + 2 :])


def collect(array, axis, dim):
    parts = sent_to_all(array, axis)
    return joined_along(parts, dim)


def of_everyone(array, axis):
    everything = sent_to_all(array, axis)
    return jnp.sum(everything.astype(jnp.float32), axis=0)


def pick_tail(history, accepted):
    rows = history.shape[1]
    keep = CONV - 1
    index = jnp.arange(rows, dtype=jnp.int32)
    offsets = jnp.arange(keep, dtype=jnp.int32)
    select = (index[None, None, :] == accepted[:, None, None] + offsets[None, :, None]).astype(
        jnp.float32
    )
    flat = history.astype(jnp.float32).reshape(history.shape[0], rows, -1)
    picked = jnp.einsum("skr,src->skc", select, flat, precision=lax.Precision.HIGHEST)
    return picked.reshape((history.shape[0], keep) + history.shape[2:])


def causal_conv(window, weight):
    length = window.shape[1] - CONV + 1
    total = weight[0] * window[:, 0:length]
    for offset in range(1, CONV):
        total = total + weight[offset] * window[:, offset : offset + length]
    return jax.nn.silu(total)


def local_mixer_output(
    unfiltered_heads,
    gate_logits,
    unfiltered_maps,
    step_logits,
    prior_heads_window,
    prior_maps_window,
    accepted,
    proposal_run,
    prior_state_value,
    previous_head_input,
    previous_input_maps,
    previous_log_decays,
    head_input_kernel,
    state_maps_kernel,
    step_size_bias,
    head_decay_speed,
    head_direct_gain,
    grouped_norm_gain,
):
    seqs, props, width = unfiltered_heads.shape
    heads = step_logits.shape[2]
    groups = unfiltered_maps.shape[3] // STATE
    repeat = heads // groups
    tail_x = pick_tail(prior_heads_window, accepted)
    tail_bc = pick_tail(prior_maps_window, accepted)
    window_x = jnp.concatenate([tail_x, unfiltered_heads.astype(jnp.float32)], axis=1)
    window_bc = jnp.concatenate([tail_bc, unfiltered_maps.astype(jnp.float32)], axis=1)
    current_heads_window = window_x.astype(jnp.bfloat16)
    current_maps_window = window_bc.astype(jnp.bfloat16)
    x_conv = causal_conv(window_x, head_input_kernel.astype(jnp.float32)).reshape(
        seqs, props, heads, HEAD_DIM
    )
    bc_conv = causal_conv(window_bc, state_maps_kernel.astype(jnp.float32)).reshape(
        seqs, props, 2, groups, STATE
    )
    b_conv = bc_conv[:, :, 0]
    c_conv = bc_conv[:, :, 1]
    positive_step_size = jax.nn.softplus(step_logits + step_size_bias)
    logarithm_decay = proposal_run - head_decay_speed * positive_step_size
    weighted = positive_step_size[..., None] * x_conv
    current_head_input = weighted.reshape(seqs, props, width).astype(jnp.bfloat16)
    current_input_maps = b_conv.reshape(seqs, props, groups * STATE).astype(jnp.bfloat16)
    past_heads = previous_head_input.astype(jnp.float32).reshape(seqs, props, heads, HEAD_DIM)
    past_keys = jnp.repeat(
        previous_input_maps.astype(jnp.float32).reshape(seqs, props, groups, STATE), repeat, axis=2
    )
    carried = prior_state_value
    for position in range(props):
        keep = (position < accepted).astype(jnp.float32)[:, None]
        factor = jnp.exp(keep * previous_log_decays[:, position])
        update = past_heads[:, position, :, :, None] * past_keys[:, position, :, None, :]
        carried = carried * factor[:, :, None, None] + keep[:, :, None, None] * update
    cumulative = jnp.cumsum(logarithm_decay, axis=1)
    c_heads = jnp.repeat(c_conv, repeat, axis=2)
    b_heads = jnp.repeat(b_conv, repeat, axis=2)
    from_state = jnp.exp(cumulative)[..., None] * jnp.einsum(
        "sthn,shpn->sthp", c_heads, carried, precision=lax.Precision.HIGHEST
    )
    order = jnp.arange(props)
    causal = (order[:, None] >= order[None, :])[None, :, :, None]
    spread_log = cumulative[:, :, None, :] - cumulative[:, None, :, :]
    decay = jnp.where(causal, jnp.exp(jnp.where(causal, spread_log, 0.0)), 0.0)
    scores = (
        jnp.einsum("sthn,suhn->stuh", c_heads, b_heads, precision=lax.Precision.HIGHEST) * decay
    )
    within = jnp.einsum("stuh,suhp->sthp", scores, weighted, precision=lax.Precision.HIGHEST)
    heads_out = from_state + within + head_direct_gain[:, None] * x_conv
    gated = heads_out.reshape(seqs, props, width) * jax.nn.silu(gate_logits)
    grouped = gated.reshape(seqs, props, groups, width // groups)
    grouped = grouped * lax.rsqrt(jnp.mean(grouped * grouped, axis=-1, keepdims=True) + eps)
    normalized_input = (
        grouped.reshape(seqs, props, width) * grouped_norm_gain.astype(jnp.float32)
    ).astype(jnp.bfloat16)
    return (
        normalized_input,
        carried,
        current_head_input,
        current_input_maps,
        logarithm_decay,
        current_heads_window,
        current_maps_window,
    )


def local(
    tokens,
    input_norm_gain,
    head_input_weight,
    output_gate_weight,
    state_maps_weight,
    step_size_weight,
    step_size_bias,
    head_decay_speed,
    proposal_decay_total,
    head_input_kernel,
    state_maps_kernel,
    head_direct_gain,
    grouped_norm_gain,
    output_weight,
    prior_state_value,
    previous_head_input,
    previous_input_maps,
    previous_log_decays,
    prior_heads_window,
    prior_maps_window,
    accepted,
):
    kv_index = lax.axis_index("kv")
    tp_index = lax.axis_index("tp")
    seq_rows, props, local_d = tokens.shape
    local_heads = step_size_weight.shape[1] // lax.axis_size("tp")
    local_width = head_input_weight.shape[1]
    local_bc = state_maps_weight.shape[2]
    own_seqs = prior_state_value.shape[0]
    own_rows = own_seqs * props
    own_start = kv_index * own_rows
    head_start = tp_index * local_heads
    values = tokens.astype(jnp.float32)
    sumsq = jnp.sum(values * values, axis=-1).reshape(seq_rows * props)
    row_total = taken_together(sumsq, "kv")
    own_sumsq = lax.dynamic_slice_in_dim(row_total, own_start, own_rows, 0)
    gain_part = lax.dynamic_slice_in_dim(input_norm_gain, kv_index * local_d, local_d, 0)
    scaled = (
        (values * gain_part.astype(jnp.float32))
        .astype(jnp.bfloat16)
        .reshape(seq_rows * props, local_d)
    )
    step_part = lax.dynamic_slice(
        step_size_weight, (kv_index * local_d, head_start), (local_d, local_heads)
    )
    proj_x = jnp.dot(scaled, head_input_weight, preferred_element_type=jnp.float32)
    proj_gate = jnp.dot(scaled, output_gate_weight, preferred_element_type=jnp.float32)
    proj_bc = jnp.dot(
        scaled, state_maps_weight.reshape(local_d, 2 * local_bc), preferred_element_type=jnp.float32
    )
    proj_step = jnp.dot(scaled, step_part, preferred_element_type=jnp.float32)
    members = (proj_x, proj_gate, proj_bc, proj_step) + ()
    summed = jax.tree.map(lambda part: summed_on_arrival(part, "kv", 0), shortened(members))
    inv_rms = lax.rsqrt(own_sumsq / D + eps)[:, None]
    unfiltered_heads = (
        (summed[0] * inv_rms).astype(jnp.bfloat16).reshape(own_seqs, props, local_width)
    )
    gate_logits = (summed[1] * inv_rms).reshape(own_seqs, props, local_width)
    unfiltered_maps = (
        (summed[2] * inv_rms).astype(jnp.bfloat16).reshape(own_seqs, props, 2, local_bc)
    )
    step_logits = (summed[3] * inv_rms).reshape(own_seqs, props, local_heads)
    bias_part = lax.dynamic_slice_in_dim(step_size_bias, head_start, local_heads, 0)
    rate_part = lax.dynamic_slice_in_dim(head_decay_speed, head_start, local_heads, 0)
    skip_part = lax.dynamic_slice_in_dim(head_direct_gain, head_start, local_heads, 0)
    conv_x_part = lax.dynamic_slice_in_dim(
        head_input_kernel, tp_index * local_width, local_width, 1
    )
    conv_bc_part = lax.dynamic_slice_in_dim(state_maps_kernel, tp_index * local_bc, local_bc, 2)
    out_gain_part = lax.dynamic_slice_in_dim(
        grouped_norm_gain, tp_index * local_width, local_width, 0
    )
    (
        normalized_input,
        accepted_state,
        current_head_input,
        current_input_maps,
        current_log_decays,
        current_heads_window,
        current_maps_window,
    ) = local_mixer_output(
        unfiltered_heads,
        gate_logits,
        unfiltered_maps,
        step_logits,
        prior_heads_window,
        prior_maps_window,
        accepted,
        proposal_decay_total,
        prior_state_value,
        previous_head_input,
        previous_input_maps,
        previous_log_decays,
        conv_x_part,
        conv_bc_part,
        bias_part,
        rate_part,
        skip_part,
        out_gain_part,
    )
    flat = normalized_input.reshape(own_rows, local_width)
    partial_value = jnp.dot(
        collect(flat, "kv", 0), output_weight, preferred_element_type=jnp.float32
    )
    mixed = (
        of_everyone(partial_value.astype(jnp.bfloat16), "tp")
        .astype(jnp.float32)
        .astype(jnp.bfloat16)
    )
    return (
        mixed.reshape(seq_rows, props, local_d),
        accepted_state,
        current_head_input,
        current_input_maps,
        current_log_decays,
        current_heads_window,
        current_maps_window,
    )


def solution(mesh):
    return jax.shard_map(
        local,
        mesh=mesh,
        in_specs=(
            P("dp", None, "kv"),
            P(),
            P("kv", "tp"),
            P("kv", "tp"),
            P("kv", None, "tp"),
            P(),
            P(),
            P(),
            P(("dp", "kv"), None, "tp"),
            P(),
            P(),
            P(),
            P(),
            P("tp", "kv"),
            P(("dp", "kv"), "tp", None, None),
            P(("dp", "kv"), None, "tp"),
            P(("dp", "kv"), None, "tp"),
            P(("dp", "kv"), None, "tp"),
            P(("dp", "kv"), None, "tp"),
            P(("dp", "kv"), None, None, "tp"),
            P(("dp", "kv")),
        ),
        out_specs=(
            P("dp", None, "kv"),
            P(("dp", "kv"), "tp", None, None),
            P(("dp", "kv"), None, "tp"),
            P(("dp", "kv"), None, "tp"),
            P(("dp", "kv"), None, "tp"),
            P(("dp", "kv"), None, "tp"),
            P(("dp", "kv"), None, None, "tp"),
        ),
        check_vma=False,
    )
```

profile of v0, /device:TPU:1, one launch (start us, length us, event | category | flops | bytes accessed | tf_op | source)
XLA Modules:
  0.0 150.1 jit_solution(2516990784292316785)
XLA Ops:
  0.7 0.8 dynamic-slice_convert_fusion.3
  1.5 1.0 fusion.6
  2.5 0.9 convolution_convert_fusion.4
  3.3 0.8 copy.207
  4.1 11.9 %all-to-all-start = ((bf16[32,8,24]{2,1,0:T(8,128)(2,1)}), bf16[32,8,24]{2,1,0:T(8,128)(2,1)S(1)}, u32[]{:S(2)}, u32[]{:S(2)}) async-start(bf16[32,8,24]{2,1,0:T(8,128)(2,1)} %bitcast.1), calls=%async_computation | async-start | bytes 131072 | tf_op jit(solution)/shard_map/all_to_all | solution.py:34
  16.0 0.7 iota_add_fusion
  17.4 0.8 fusion.39
  18.2 0.9 copy.241
  19.1 1.1 fusion.2
  20.2 1.3 fusion.1
  21.5 1.3 fusion
  23.0 1.8 %all-to-all-done = bf16[32,8,24]{2,1,0:T(8,128)(2,1)S(1)} async-done(((bf16[32,8,24]{2,1,0:T(8,128)(2,1)}), bf16[32,8,24]{2,1,0:T(8,128)(2,1)S(1)}, u32[]{:S(2)}, u32[]{:S(2)}) %all-to-all-start) | async-done | bytes 12320 | tf_op jit(solution)/shard_map/all_to_all | solution.py:34
  25.4 7.5 %all-to-all-start.1 = ((f32[32,1,256]{2,1,0:T(1,128)}), f32[32,1,256]{2,1,0:T(1,128)S(1)}, u32[]{:S(2)}, u32[]{:S(2)}) async-start(f32[32,1,256]{2,1,0:T(1,128)} %broadcast_in_dim.29), calls=%async_computation.1 | async-start | bytes 65536 | tf_op jit(solution)/shard_map/all_to_all | solution.py:17
  33.6 8.0 %all-to-all-done.1 = f32[32,1,256]{2,1,0:T(1,128)S(1)} async-done(((f32[32,1,256]{2,1,0:T(1,128)}), f32[32,1,256]{2,1,0:T(1,128)S(1)}, u32[]{:S(2)}, u32[]{:S(2)}) %all-to-all-start.1) | async-done | bytes 32800 | tf_op jit(solution)/shard_map/all_to_all | solution.py:17
  41.6 3.9 %all-to-all-start.2 = ((bf16[32,8,1024]{2,1,0:T(8,128)(2,1)}), bf16[32,8,1024]{2,1,0:T(8,128)(2,1)S(1)}, u32[]{:S(2)}, u32[]{:S(2)}) async-start(bf16[32,8,1024]{2,1,0:T(8,128)(2,1)} %fusion.2), calls=%async_computation.2 | async-start | bytes 1048576 | tf_op jit(solution)/shard_map/all_to_all | solution.py:34
  47.1 12.6 %all-to-all-done.2 = bf16[32,8,1024]{2,1,0:T(8,128)(2,1)S(1)} async-done(((bf16[32,8,1024]{2,1,0:T(8,128)(2,1)}), bf16[32,8,1024]{2,1,0:T(8,128)(2,1)S(1)}, u32[]{:S(2)}, u32[]{:S(2)}) %all-to-all-start.2) | async-done | bytes 524320 | tf_op jit(solution)/shard_map/all_to_all | solution.py:34
  59.7 0.8 copy-done.2
  60.5 5.9 %all-to-all-start.4 = ((bf16[32,8,1536]{2,1,0:T(8,128)(2,1)}), bf16[32,8,1536]{2,1,0:T(8,128)(2,1)S(1)}, u32[]{:S(2)}, u32[]{:S(2)}) async-start(bf16[32,8,1536]{2,1,0:T(8,128)(2,1)} %fusion.1), calls=%async_computation.4 | async-start | bytes 1572864 | tf_op jit(solution)/shard_map/all_to_all | solution.py:34
  69.2 4.0 %multiply_add_fusion = f32[2,24,64,128]{3,2,1,0:T(8,128)S(1)} fusion(f32[2,24,64,128]{3,2,1,0:T(8,128)} %param.35, f32[2,24,128]{2,1,0:T(8,128)S(1)} %bitcast.104, f32[2,24,64]{2,1,0:T(8,128)S(1)} %get-tuple-element.83, f32[2]{0:T(128)S(1)} %get-tuple-element.103, f32[2,24]{1,0:T(2,128)S(1)} %get-tuple-element.104, f32[2,24,128]{2,1,0:T(8,128)S(1)} %bitcast.105, ...), kind=kLoop, calls=%fused_computation.6 | loop fusion | flops 6291456 | bytes 3293984 | tf_op jit(solution)/shard_map/add | solution.py:135
  73.5 11.5 %all-to-all-done.4 = bf16[32,8,1536]{2,1,0:T(8,128)(2,1)S(1)} async-done(((bf16[32,8,1536]{2,1,0:T(8,128)(2,1)}), bf16[32,8,1536]{2,1,0:T(8,128)(2,1)S(1)}, u32[]{:S(2)}, u32[]{:S(2)}) %all-to-all-start.4) | async-done | bytes 786464 | tf_op jit(solution)/shard_map/all_to_all | solution.py:34
  85.0 7.2 %all-to-all-start.3 = ((bf16[32,8,1536]{2,1,0:T(8,128)(2,1)}), bf16[32,8,1536]{2,1,0:T(8,128)(2,1)S(1)}, u32[]{:S(2)}, u32[]{:S(2)}) async-start(bf16[32,8,1536]{2,1,0:T(8,128)(2,1)} %fusion), calls=%async_computation.3 | async-start | bytes 1572864 | tf_op jit(solution)/shard_map/all_to_all | solution.py:34
  93.8 0.7 mul.552
  94.5 1.1 convert_reduce_fusion.2
  95.7 0.8 divide_multiply_fusion.1
  97.2 1.9 %fusion.3 = f32[2,4,4,24]{1,2,3,0:T(4,128)} fusion(f32[2,4,24,128]{3,1,2,0:T(4,128)S(1)} %bitcast.107, f32[2,4,24,128]{3,1,2,0:T(4,128)S(1)} %bitcast.98, f32[2,4,24]{1,2,0:T(8,128)} %copy.222, pred[4,4]{0,1:T(4,128)(4,1)} %iota_compare_fusion.3), kind=kOutput, calls=%fused_computation.10 | convolution fusion | flops 1182720 | bytes 200464 | tf_op jit(solution)/shard_map/sthn,suhn->stuh/dot_general | solution.py:147
  99.1 2.5 %fusion.40 = f32[2,24,64,4]{2,3,1,0:T(4,128)S(1)} fusion(f32[2,24,64,128]{3,2,1,0:T(8,128)S(1)} %multiply_add_fusion, f32[2,4,24,128]{3,1,2,0:T(4,128)S(1)} %bitcast.99), kind=kOutput, calls=%fused_computation.111 | convolution fusion | flops 18874368 | bytes 1720320 | tf_op jit(solution)/shard_map/sthn,shpn->sthp/dot_general | solution.py:139
  101.9 8.9 %all-to-all-done.3 = bf16[32,8,1536]{2,1,0:T(8,128)(2,1)S(1)} async-done(((bf16[32,8,1536]{2,1,0:T(8,128)(2,1)}), bf16[32,8,1536]{2,1,0:T(8,128)(2,1)S(1)}, u32[]{:S(2)}, u32[]{:S(2)}) %all-to-all-start.3) | async-done | bytes 786464 | tf_op jit(solution)/shard_map/all_to_all | solution.py:34
  113.3 1.0 broadcast_in_dim.39
  114.3 7.2 %all-to-all-start.5 = ((bf16[32,8,1536]{2,1,0:T(8,128)(2,1)}), bf16[32,8,1536]{2,1,0:T(8,128)(2,1)S(1)}, u32[]{:S(2)}, u32[]{:S(2)}) async-start(bf16[32,8,1536]{2,1,0:T(8,128)(2,1)} %broadcast_in_dim.39), calls=%async_computation.5 | async-start | bytes 1572864 | tf_op jit(solution)/shard_map/all_to_all | solution.py:17
  124.1 16.0 %all-to-all-done.5 = bf16[32,8,1536]{2,1,0:T(8,128)(2,1)S(1)} async-done(((bf16[32,8,1536]{2,1,0:T(8,128)(2,1)}), bf16[32,8,1536]{2,1,0:T(8,128)(2,1)S(1)}, u32[]{:S(2)}, u32[]{:S(2)}) %all-to-all-start.5) | async-done | bytes 786464 | tf_op jit(solution)/shard_map/all_to_all | solution.py:17
  140.5 8.9 %all_to_all.36 = bf16[2,256,64]{1,2,0:T(8,128)(2,1)S(1)} all-to-all(bf16[2,256,64]{1,2,0:T(8,128)(2,1)S(1)} %broadcast_in_dim.40), channel_id=1, replica_groups=mesh['dp'=4,'kv'=32,'tp'=2] {'tp'}, dimensions={0} | all-to-all | bytes 131072 | tf_op jit(solution)/shard_map/all_to_all | solution.py:17
  149.4 0.7 copy.229
  (126 shorter events, 14.7 us)
Async XLA Ops:
  0.6 19.6 %copy-start = (bf16[64,1536]{1,0:T(8,128)(2,1)S(1)}, bf16[64,1536]{1,0:T(8,128)(2,1)}, u32[]{:S(2)}) copy-start(bf16[64,1536]{1,0:T(8,128)(2,1)} %param.24) | copy-start | bytes 589828
  0.6 20.8 %copy-start.3 = (bf16[64,1536]{1,0:T(8,128)(2,1)S(1)}, bf16[64,1536]{1,0:T(8,128)(2,1)}, u32[]{:S(2)}) copy-start(bf16[64,1536]{1,0:T(8,128)(2,1)} %param.23) | copy-start | bytes 589828
  4.1 20.7 %all-to-all-start = ((bf16[32,8,24]{2,1,0:T(8,128)(2,1)}), bf16[32,8,24]{2,1,0:T(8,128)(2,1)S(1)}, u32[]{:S(2)}, u32[]{:S(2)}) async-start(bf16[32,8,24]{2,1,0:T(8,128)(2,1)} %bitcast.1), calls=%async_computation | async-start | bytes 131072 | tf_op jit(solution)/shard_map/all_to_all | solution.py:34
  16.0 6.8 %copy-start.19 = (bf16[4,3072]{1,0:T(4,128)(2,1)S(1)}, bf16[4,3072]{1,0:T(4,128)(2,1)}, u32[]{:S(2)}) copy-start(bf16[4,3072]{1,0:T(4,128)(2,1)} %param.30) | copy-start | bytes 73732
  19.1 13.7 %copy-start.22 = (bf16[3072]{0:T(1024)(128)(2,1)S(1)}, bf16[3072]{0:T(1024)(128)(2,1)}, u32[]{:S(2)}) copy-start(bf16[3072]{0:T(1024)(128)(2,1)} %param.33) | copy-start | bytes 18436
  22.7 44.2 %copy-start.28 = (f32[48]{0:T(128)S(1)}, f32[48]{0:T(128)}, u32[]{:S(2)}) copy-start(f32[48]{0:T(128)} %param.27) | copy-start | bytes 580
  22.7 44.8 %copy-start.29 = (f32[48]{0:T(128)S(1)}, f32[48]{0:T(128)}, u32[]{:S(2)}) copy-start(f32[48]{0:T(128)} %param.28) | copy-start | bytes 580
  22.8 45.3 %copy-start.30 = (f32[48]{0:T(128)S(1)}, f32[48]{0:T(128)}, u32[]{:S(2)}) copy-start(f32[48]{0:T(128)} %param.32) | copy-start | bytes 580
  22.8 46.0 %copy-start.15 = (bf16[2,4,1536]{2,1,0:T(4,128)(2,1)S(1)}, bf16[2,4,1536]{2,1,0:T(4,128)(2,1)}, u32[]{:S(2)}) copy-start(bf16[2,4,1536]{2,1,0:T(4,128)(2,1)} %param.36) | copy-start | bytes 73732
  22.9 46.0 %copy-start.18 = (bf16[2,4,512]{2,1,0:T(4,128)(2,1)S(1)}, bf16[2,4,512]{2,1,0:T(4,128)(2,1)}, u32[]{:S(2)}) copy-start(bf16[2,4,512]{2,1,0:T(4,128)(2,1)} %param.37) | copy-start | bytes 24580
  23.0 45.9 %copy-start.8 = (bf16[2,7,1536]{2,0,1:T(2,128)(2,1)S(1)}, bf16[2,7,1536]{2,0,1:T(2,128)(2,1)}, u32[]{:S(2)}) copy-start(bf16[2,7,1536]{2,0,1:T(2,128)(2,1)} %param.39) | copy-start | bytes 129028
  25.4 16.2 %all-to-all-start.1 = ((f32[32,1,256]{2,1,0:T(1,128)}), f32[32,1,256]{2,1,0:T(1,128)S(1)}, u32[]{:S(2)}, u32[]{:S(2)}) async-start(f32[32,1,256]{2,1,0:T(1,128)} %broadcast_in_dim.29), calls=%async_computation.1 | async-start | bytes 65536 | tf_op jit(solution)/shard_map/all_to_all | solution.py:17
  41.6 18.1 %all-to-all-start.2 = ((bf16[32,8,1024]{2,1,0:T(8,128)(2,1)}), bf16[32,8,1024]{2,1,0:T(8,128)(2,1)S(1)}, u32[]{:S(2)}, u32[]{:S(2)}) async-start(bf16[32,8,1024]{2,1,0:T(8,128)(2,1)} %fusion.2), calls=%async_computation.2 | async-start | bytes 1048576 | tf_op jit(solution)/shard_map/all_to_all | solution.py:34
  60.5 24.5 %all-to-all-start.4 = ((bf16[32,8,1536]{2,1,0:T(8,128)(2,1)}), bf16[32,8,1536]{2,1,0:T(8,128)(2,1)S(1)}, u32[]{:S(2)}, u32[]{:S(2)}) async-start(bf16[32,8,1536]{2,1,0:T(8,128)(2,1)} %fusion.1), calls=%async_computation.4 | async-start | bytes 1572864 | tf_op jit(solution)/shard_map/all_to_all | solution.py:34
  73.2 25.9 %copy-start.1 = (f32[2,24,64,128]{3,2,1,0:T(8,128)}, f32[2,24,64,128]{3,2,1,0:T(8,128)S(1)}, u32[]{:S(2)}) copy-start(f32[2,24,64,128]{3,2,1,0:T(8,128)S(1)} %multiply_add_fusion) | copy-start | bytes 4718596
  73.2 19.0 %copy-start.21 = (f32[2,4,24]{2,1,0:T(4,128)S(1)}, f32[2,4,24]{2,1,0:T(4,128)}, u32[]{:S(2)}) copy-start(f32[2,4,24]{2,1,0:T(4,128)} %param.29) | copy-start | bytes 2308
  73.2 19.0 %copy-start.26 = (f32[24]{0:T(128)S(1)}, f32[24]{0:T(128)}, u32[]{:S(2)}) copy-start(f32[24]{0:T(128)} %dynamic_slice.31) | copy-start | bytes 292
  73.2 19.0 %copy-start.27 = (f32[24]{0:T(128)S(1)}, f32[24]{0:T(128)}, u32[]{:S(2)}) copy-start(f32[24]{0:T(128)} %dynamic_slice.27) | copy-start | bytes 292
  73.4 18.8 %copy-start.24 = (f32[8]{0:T(128)}, f32[8]{0:T(128)S(1)}, u32[]{:S(2)}) copy-start(f32[8]{0:T(128)S(1)} %add_rsqrt_fusion.1) | copy-start | bytes 100
  85.0 25.8 %all-to-all-start.3 = ((bf16[32,8,1536]{2,1,0:T(8,128)(2,1)}), bf16[32,8,1536]{2,1,0:T(8,128)(2,1)S(1)}, u32[]{:S(2)}, u32[]{:S(2)}) async-start(bf16[32,8,1536]{2,1,0:T(8,128)(2,1)} %fusion), calls=%async_computation.3 | async-start | bytes 1572864 | tf_op jit(solution)/shard_map/all_to_all | solution.py:34
  101.6 9.4 %copy-start.4 = (f32[2,4,1536]{2,1,0:T(4,128)S(1)}, f32[2,4,1536]{2,1,0:T(4,128)}, u32[]{:S(2)}) copy-start(f32[2,4,1536]{2,1,0:T(4,128)} %mul.552) | copy-start | bytes 147460
  101.6 9.4 %copy-start.9 = (f32[1536]{0:T(1024)S(1)}, f32[1536]{0:T(1024)}, u32[]{:S(2)}) copy-start(f32[1536]{0:T(1024)} %get-tuple-element.70) | copy-start | bytes 18436
  101.6 9.4 %copy-start.10 = (f32[1536]{0:T(1024)S(1)}, f32[1536]{0:T(1024)}, u32[]{:S(2)}) copy-start(f32[1536]{0:T(1024)} %get-tuple-element.71) | copy-start | bytes 18436
  101.6 9.4 %copy-start.11 = (f32[1536]{0:T(1024)S(1)}, f32[1536]{0:T(1024)}, u32[]{:S(2)}) copy-start(f32[1536]{0:T(1024)} %get-tuple-element.72) | copy-start | bytes 18436
  101.7 9.4 %copy-start.12 = (f32[1536]{0:T(1024)S(1)}, f32[1536]{0:T(1024)}, u32[]{:S(2)}) copy-start(f32[1536]{0:T(1024)} %get-tuple-element.73) | copy-start | bytes 18436
  101.7 10.3 %copy-start.7 = (f32[2,4,4,24]{1,2,3,0:T(4,128)S(1)}, f32[2,4,4,24]{1,2,3,0:T(4,128)}, u32[]{:S(2)}) copy-start(f32[2,4,4,24]{1,2,3,0:T(4,128)} %fusion.3) | copy-start | bytes 9220
  101.7 10.9 %copy-start.16 = (f32[2,4,24]{2,1,0:T(4,128)S(1)}, f32[2,4,24]{2,1,0:T(4,128)}, u32[]{:S(2)}) copy-start(f32[2,4,24]{2,1,0:T(4,128)} %exp.67) | copy-start | bytes 2308
  101.7 10.9 %copy-start.23 = (f32[24]{0:T(128)S(1)}, f32[24]{0:T(128)}, u32[]{:S(2)}) copy-start(f32[24]{0:T(128)} %dynamic_slice.34) | copy-start | bytes 292
  101.8 11.4 %copy-start.13 = (f32[1536]{0:T(1024)S(1)}, f32[1536]{0:T(1024)}, u32[]{:S(2)}) copy-start(f32[1536]{0:T(1024)} %dynamic-slice_convert_fusion.2) | copy-start | bytes 18436
  101.8 11.4 %copy-start.25 = (f32[8]{0:T(128)S(1)}, f32[8]{0:T(128)}, u32[]{:S(2)}) copy-start(f32[8]{0:T(128)} %copy-done.24) | copy-start | bytes 100
  113.0 27.1 %copy-start.5 = (bf16[1536,64]{0,1:T(8,128)(2,1)S(1)}, bf16[1536,64]{0,1:T(8,128)(2,1)}, u32[]{:S(2)}) copy-start(bf16[1536,64]{0,1:T(8,128)(2,1)} %param.34) | copy-start | bytes 589828
  114.3 25.9 %all-to-all-start.5 = ((bf16[32,8,1536]{2,1,0:T(8,128)(2,1)}), bf16[32,8,1536]{2,1,0:T(8,128)(2,1)S(1)}, u32[]{:S(2)}, u32[]{:S(2)}) async-start(bf16[32,8,1536]{2,1,0:T(8,128)(2,1)} %broadcast_in_dim.39), calls=%async_computation.5 | async-start | bytes 1572864 | tf_op jit(solution)/shard_map/all_to_all | solution.py:17
  (5 other events, 12.8 us)
where the time goes:
time: 151 us; the launch traced here: 150 us
  waiting for transfers between devices  58.7 us (39%)
  starting transfers between devices  43.5 us (29%)
  local copies, waits for them, and re-layouts  14.5 us (10%)
  other arithmetic  13 us (9%)
  matrix products  10.2 us (7%)
  blocking collectives  8.91 us (6%)
    all_to_all x4, waiting for transfers between devices, summed_on_arrival(): lax.all_to_all(parts, axis, split_axis=0, concat_axis=0, tiled=True)  34.7 us
    all_to_all x4, starting transfers between devices, summed_on_arrival(): lax.all_to_all(parts, axis, split_axis=0, concat_axis=0, tiled=True)  28.9 us
    all_to_all x2, waiting for transfers between devices, sent_to_all(): lax.all_to_all(jnp.broadcast_to(array[None], (devices, *array.shape)), ax...  24 us
    all_to_all x2, starting transfers between devices, sent_to_all(): lax.all_to_all(jnp.broadcast_to(array[None], (devices, *array.shape)), ax...  14.6 us
    all_to_all x1, blocking collectives, sent_to_all(): lax.all_to_all(jnp.broadcast_to(array[None], (devices, *array.shape)), ax...  8.91 us
    add x1, other arithmetic, local_mixer_output(): carried * factor[:, :, None, None] + keep[:, :, None, None] * update  3.97 us
    unnamed x65, local copies, waits for them, and re-layouts  3.06 us
  transfers between devices with their start and end apart: 6, of which 6 were waited for; matrix products, arithmetic and copies ran while one was open for 19% of the time, Pallas kernels for 0%

commit v1 on v0

v1 whole, which is shorter than its diff:
```python
import functools

import jax
import jax.numpy as jnp
from jax import lax
from jax.experimental import pallas as pl
from jax.experimental.pallas import tpu as pltpu
from jax.sharding import PartitionSpec as P

MESH = pl.DeviceIdType.MESH
HI = lax.Precision.HIGHEST
f32, bf16, i32 = jnp.float32, jnp.bfloat16, jnp.int32

NX, NZ, NT = 4, 8, 2
PEERS = NX * NZ
D, STATE, HEAD_DIM = 2048, 128, 64
SEQS, PROPS, ROWS = 2, 4, 8
HEADS, GROUPS, PER = 24, 4, 6
WIDTH, GW = 1536, 384
BC = 512
eps = 1e-06


def iota(shape, dim):
    return lax.broadcasted_iota(i32, shape, dim)


def mm(a, b, ca=1, cb=0, precision=None):
    return lax.dot_general(
        a, b, (((ca,), (cb,)), ((), ())), precision=precision, preferred_element_type=f32
    )


def heads_selection(acc):
    shape = (48, 24)
    i, j = iota(shape, 0), iota(shape, 1)
    out = i >= 32
    b = jnp.where(out, i & 1, (i >> 2) & 1)
    pos = jnp.where(out, (i - 32) >> 1, (i & 3) + (i >> 3))
    acc_b = jnp.where(b == 0, acc[0], acc[1])
    old = (j < 14) & ((j & 1) == b) & ((j >> 1) == acc_b + pos)
    raw = (j >= 16) & (((j - 16) >> 2) == b) & (((j - 16) & 3) == pos - 3)
    pick = jnp.where(pos < 3, jnp.where(old, 1.0, 0.0), jnp.where(raw, 1.0, 0.0))
    return pick.astype(bf16)


def maps_selection(acc):
    shape = (96, 48)
    i, j = iota(shape, 0), iota(shape, 1)
    out = i >= 64
    o = i - 64
    ob = jnp.where(o >= 14, 1, 0)
    orem = o - 14 * ob
    b = jnp.where(out, ob, (i >> 2) & 1)
    pos = jnp.where(out, orem >> 1, (i & 3) + (i >> 4))
    kind = jnp.where(out, orem & 1, (i >> 3) & 1)
    acc_b = jnp.where(b == 0, acc[0], acc[1])
    jb = jnp.where(j >= 14, 1, 0)
    jrem = j - 14 * jb
    old = (j < 28) & (jb == b) & ((jrem & 1) == kind) & ((jrem >> 1) == acc_b + pos)
    jr = j - 32
    raw = (j >= 32) & ((jr >> 3) == kind) & (((jr >> 2) & 1) == b) & ((jr & 3) == pos - 3)
    pick = jnp.where(pos < 3, jnp.where(old, 1.0, 0.0), jnp.where(raw, 1.0, 0.0))
    return pick.astype(bf16)


def kernel(
    tok_h, gain_h, wx_h, wg_h, smw_h, sw_h, ssb_h, hds_h, pdt_h, hik_h, smk_h, hdg_h, gng_h, wo_h,
    psv_h, phi_h, pim_h, pld_h, phw_h, pmw_h, acc_s,
    mixed_o, state_o, chi_o, cim_o, cld_o, chw_o, cmw_o,
    tok, gain, wx, wg, smw, ssb, hds, pdt, hik, smk, hdg, gng, wo, psv, phi, pim, pld, phw, pmw,
    sw, bcs, tt, wb, wxr, wgr, s0, s1, s2, r0, r1, r2, wor, sb, nrm, fs, fr,
    lsem, ssem, rsem, osem,
):
    y, kv, t = lax.axis_index("dp"), lax.axis_index("kv"), lax.axis_index("tp")
    z, x = kv // NX, kv % NX

    def at(zz, xx, tt_):
        return dict(device_id=(y, zz * NX + xx, tt_), device_id_type=MESH)

    loads = {}
    plan = (
        (tok_h, tok), (gain_h, gain), (smw_h, smw), (wx_h, wx), (wg_h, wg),
        (sw_h.at[:, pl.ds(pl.multiple_of(z * 256, 256), 256)], sw.at[pl.ds(0, 48)]),
        (ssb_h, ssb), (hds_h, hds), (pdt_h, pdt),
        (hik_h.at[:, pl.ds(pl.multiple_of(t * WIDTH, 128), WIDTH)], hik),
        (smk_h.at[:, :, pl.ds(pl.multiple_of(t * BC, 128), BC)], smk),
        (hdg_h, hdg), (gng_h, gng), (wo_h, wo), (phi_h, phi), (pim_h, pim), (pld_h, pld),
        (phw_h, phw), (pmw_h, pmw), (psv_h, psv),
    )
    for n, (src, dst) in enumerate(plan):
        loads[n] = pltpu.make_async_copy(src, dst, lsem.at[n])
        loads[n].start()

    barrier = pltpu.get_barrier_semaphore()

    def greet(d, _):
        other = lax.rem(kv + d, PEERS)
        pl.semaphore_signal(barrier, inc=1, device_id=(y, other, t), device_id_type=MESH)
        return 0

    lax.fori_loop(1, PEERS, greet, 0)
    for d in range(NX):
        pl.semaphore_signal(barrier, inc=1, **at(z, lax.rem(x + d, NX), 1 - t))

    for n in (0, 1, 2):
        loads[n].wait()
    tok32 = tok[...].astype(f32).reshape(256, 64)
    sumsq = jnp.sum(tok32 * tok32, axis=1, keepdims=True)
    gains = gain[...].astype(f32).reshape(16, 128)
    gain_row = jnp.sum(
        jnp.where(iota((16, 128), 0) == kv // 2, gains, 0.0), axis=0, keepdims=True
    )
    gain_row = jnp.where(kv % 2 == 0, gain_row[:, :64], gain_row[:, 64:])
    tt[x] = (tok32 * gain_row).astype(bf16).T
    b_w, c_w = smw[:, 0, :], smw[:, 1, :]
    for g in range(GROUPS):
        bcs[g, :, 0:128] = b_w[:, g * 128 : g * 128 + 128]
        bcs[g, :, 128:256] = c_w[:, g * 128 : g * 128 + 128]
    wb[x] = bcs[x]
    sw[48:128] = jnp.zeros((80, 256), bf16)
    loads[3].wait()
    loads[4].wait()
    own = pl.ds(pl.multiple_of(x * GW, 128), GW)
    wxr[x] = wx[:, own]
    wgr[x] = wg[:, own]

    pl.semaphore_wait(barrier, PEERS - 1 + NX)

    for n, d in enumerate((2, 1, 3)):
        xp = lax.rem(x + d, NX)
        pltpu.make_async_remote_copy(
            tt.at[x], tt.at[x], ssem.at[0], rsem.at[0], **at(z, xp, t)
        ).start()
        pltpu.make_async_remote_copy(
            bcs.at[xp], wb.at[x], ssem.at[1], rsem.at[1], **at(z, xp, t)
        ).start()
    for n, (src, dst) in enumerate(((wx, wxr), (wg, wgr))):
        for d in (2, 1, 3):
            xp = lax.rem(x + d, NX)
            pltpu.make_async_remote_copy(
                src.at[:, pl.ds(pl.multiple_of(xp * GW, 128), GW)],
                dst.at[x],
                ssem.at[2 + n],
                rsem.at[2 + n],
                **at(z, xp, t),
            ).start()

    def arrived(buffer, count, sem):
        block = buffer.at[pl.ds(0, count)]
        pltpu.make_async_copy(block, block, sem).wait()

    def spread(c, src, dst):
        def one(d, _):
            other = lax.rem(kv + d, PEERS)
            pltpu.make_async_remote_copy(
                src.at[other],
                dst.at[x * NZ + z],
                ssem.at[4 + c],
                rsem.at[4 + c],
                device_id=(y, other, t),
                device_id_type=MESH,
            ).start()
            return 0

        lax.fori_loop(1, PEERS, one, 0)
        dst[x * NZ + z] = src[kv]

    loads[5].wait()
    arrived(tt, 3, rsem.at[0])
    arrived(wb, 3, rsem.at[1])
    lhs = tt[...].reshape(256, 256)
    part = mm(lhs, wb[...].reshape(256, 256), 0, 0)
    steps = mm(lhs, sw[...], 0, 1)
    high = sumsq.astype(bf16).astype(f32)
    lane = iota((256, 128), 1)
    steps = jnp.where(lane == 64, high, jnp.where(lane == 65, sumsq - high, steps))
    s0[:, :, 0:256] = part.reshape(PEERS, ROWS, 256).astype(bf16)
    s0[:, :, 256:384] = steps.reshape(PEERS, ROWS, 128).astype(bf16)
    spread(0, s0, r0)
    arrived(wxr, 3, rsem.at[2])
    s1[...] = mm(tt[...].reshape(256, 256), wxr[...].reshape(256, GW), 0, 0).reshape(
        PEERS, ROWS, GW
    ).astype(bf16)
    spread(1, s1, r1)
    arrived(wgr, 3, rsem.at[3])
    s2[...] = mm(tt[...].reshape(256, 256), wgr[...].reshape(256, GW), 0, 0).reshape(
        PEERS, ROWS, GW
    ).astype(bf16)
    spread(2, s2, r2)
    loads[13].wait()
    wor[x] = wo[...]
    for d in (2, 1, 3):
        pltpu.make_async_remote_copy(
            wo, wor.at[x], ssem.at[7], rsem.at[7], **at(z, lax.rem(x + d, NX), t)
        ).start()

    acc = (acc_s[0], acc_s[1])
    row = iota((ROWS, 1), 0)
    acc_row = jnp.where(row < PROPS, acc[0], acc[1])
    keep = jnp.where((row & 3) < acc_row, 1.0, 0.0)
    r8, c8 = iota((ROWS, ROWS), 0), iota((ROWS, ROWS), 1)
    same = (r8 >> 2) == (c8 >> 2)
    expand = jnp.where(iota((HEADS, WIDTH), 1) // HEAD_DIM == iota((HEADS, WIDTH), 0), 1.0, 0.0)
    for n in (14, 15, 16):
        loads[n].wait()
    kept = pld[...].reshape(ROWS, HEADS) * keep
    later = mm(jnp.where(same & (c8 > r8), 1.0, 0.0), kept, precision=HI)
    coef = mm(keep * jnp.exp(later), expand, precision=HI)
    scaled = coef * phi[...].astype(f32).reshape(ROWS, WIDTH)
    s_hi = scaled.astype(bf16)
    s_lo = (scaled - s_hi.astype(f32)).astype(bf16)
    updates = jnp.concatenate([s_hi.astype(f32), s_lo.astype(f32)], axis=0).astype(bf16)
    keys = pim[...].astype(f32).reshape(ROWS, BC)
    loads[19].wait()
    for b in range(SEQS):
        mine = (row >> 2) == b
        logs = mm(jnp.where(mine, kept, 0.0), jnp.ones((ROWS, STATE), f32), 0, 0, precision=HI)
        factor = jnp.exp(logs)
        keys_b = jnp.where(mine, keys, 0.0)
        keys_b = jnp.concatenate([keys_b, keys_b], axis=0).astype(bf16)
        for g in range(GROUPS):
            upd = mm(
                updates[:, g * GW : g * GW + GW], keys_b[:, g * STATE : g * STATE + STATE], 0, 0
            )
            new = (
                psv[b, g * PER : g * PER + PER] * factor[g * PER : g * PER + PER][:, None, :]
                + upd.reshape(PER, HEAD_DIM, STATE)
            )
            psv[b, g * PER : g * PER + PER] = new
            sb[b, g] = new.reshape(GW, STATE).astype(bf16)
    state_out = pltpu.make_async_copy(psv, state_o, osem.at[0])
    state_out.start()

    pick_x, pick_bc = heads_selection(acc), maps_selection(acc)
    for n in (6, 7, 8, 9, 10, 11, 12, 17, 18):
        loads[n].wait()
    old_x = phw[...].astype(f32).reshape(14, WIDTH)
    old_x = jnp.concatenate([old_x, jnp.zeros((2, WIDTH), f32)], axis=0)
    old_bc = pmw[...].astype(f32).reshape(28, BC)
    old_bc = jnp.concatenate([old_bc, jnp.zeros((4, BC), f32)], axis=0)
    taps_x = hik[...].astype(f32)
    taps_bc = smk[...].astype(f32).reshape(8, BC)

    def own_heads(ref):
        v = ref[...].reshape(1, 2 * HEADS)
        return jnp.where(t == 0, v[:, :HEADS], v[:, HEADS:])

    speed, direct, bias = own_heads(hds), own_heads(hdg), own_heads(ssb)
    gngv = gng[...].astype(f32).reshape(1, 2 * WIDTH)
    out_gain = jnp.where(t == 0, gngv[:, :WIDTH], gngv[:, WIDTH:])

    arrived(r0, PEERS - 1, rsem.at[4])
    sum0 = jnp.sum(r0[...].astype(f32).reshape(NX, NZ, ROWS, GW), axis=1)
    tail = sum0[:, :, 256:384]
    squares = jnp.sum(tail, axis=0)
    lane8 = iota((ROWS, 128), 1)
    squares = jnp.sum(
        jnp.where((lane8 == 64) | (lane8 == 65), squares, 0.0), axis=1, keepdims=True
    )
    inv = lax.rsqrt(squares / D + eps)
    raw_b = jnp.concatenate([sum0[g, :, 0:128] for g in range(GROUPS)], axis=1) * inv
    raw_c = jnp.concatenate([sum0[g, :, 128:256] for g in range(GROUPS)], axis=1) * inv
    win_bc = mm(pick_bc, jnp.concatenate([old_bc, raw_b, raw_c], axis=0).astype(bf16))
    cmw_v = win_bc[64:92].reshape(SEQS, 7, 2, BC).astype(bf16)
    b_conv = taps_bc[0:1] * win_bc[0:8]
    c_conv = taps_bc[1:2] * win_bc[8:16]
    for k in range(1, 4):
        b_conv = b_conv + taps_bc[2 * k : 2 * k + 1] * win_bc[16 * k : 16 * k + 8]
        c_conv = c_conv + taps_bc[2 * k + 1 : 2 * k + 2] * win_bc[16 * k + 8 : 16 * k + 16]
    b_conv = b_conv * lax.logistic(b_conv)
    c_conv = c_conv * lax.logistic(c_conv)
    step_pre = tail[0] * inv
    step_pre = jnp.where(t == 0, step_pre[:, :HEADS], step_pre[:, HEADS : 2 * HEADS]) + bias
    step = jnp.maximum(step_pre, 0.0) + jnp.log1p(jnp.exp(-jnp.abs(step_pre)))
    decays = pdt[...].reshape(ROWS, HEADS) - speed * step
    cum = mm(jnp.where(same & (c8 <= r8), 1.0, 0.0), decays, precision=HI)
    wide = mm(
        jnp.concatenate([cum, step, jnp.broadcast_to(direct, (ROWS, HEADS))], axis=0),
        expand,
        precision=HI,
    )
    cum_w, step_w, direct_w = wide[0:8], wide[8:16], wide[16:24]
    cim_o[...] = b_conv.reshape(SEQS, PROPS, BC).astype(bf16)
    cld_o[...] = decays.reshape(SEQS, PROPS, HEADS)
    cmw_o[...] = cmw_v
    from_state, pairs = [], []
    for g in range(GROUPS):
        lanes = slice(g * STATE, g * STATE + STATE)
        c_g = c_conv[:, lanes]
        y0 = mm(c_g.astype(bf16), sb[0, g], 1, 1)
        y1 = mm(c_g.astype(bf16), sb[1, g], 1, 1)
        from_state.append(jnp.where(row < PROPS, y0, y1))
        pairs.append(mm(c_g, b_conv[:, lanes], 1, 1, precision=HI))
    from_state = jnp.exp(cum_w) * jnp.concatenate(from_state, axis=1)

    arrived(r1, PEERS - 1, rsem.at[5])
    sum1 = jnp.sum(r1[...].astype(f32).reshape(NX, NZ, ROWS, GW), axis=1)
    raw_x = jnp.concatenate([sum1[g] for g in range(GROUPS)], axis=1) * inv
    win_x = mm(pick_x, jnp.concatenate([old_x, raw_x], axis=0).astype(bf16))
    chw_o[...] = win_x[32:46].reshape(7, SEQS, WIDTH).astype(bf16)
    x_conv = taps_x[0:1] * win_x[0:8]
    for k in range(1, 4):
        x_conv = x_conv + taps_x[k : k + 1] * win_x[8 * k : 8 * k + 8]
    x_conv = x_conv * lax.logistic(x_conv)
    weighted = step_w * x_conv
    chi_o[...] = weighted.reshape(SEQS, PROPS, WIDTH).astype(bf16)
    total = from_state + direct_w * x_conv
    for d in range(PROPS):
        score = [
            jnp.broadcast_to(
                jnp.sum(jnp.where(c8 == r8 - d, p, 0.0), axis=1, keepdims=True), (ROWS, GW)
            )
            for p in pairs
        ]
        score = jnp.concatenate(score, axis=1)
        if d == 0:
            total = total + score * weighted
        else:
            valid = (row & 3) >= d
            gap = jnp.where(valid, cum_w - pltpu.roll(cum_w, d, 0), 0.0)
            term = jnp.exp(gap) * score * pltpu.roll(weighted, d, 0)
            total = total + jnp.where(valid, term, 0.0)

    arrived(r2, PEERS - 1, rsem.at[6])
    sum2 = jnp.sum(r2[...].astype(f32).reshape(NX, NZ, ROWS, GW), axis=1)
    gate = jnp.concatenate([sum2[g] for g in range(GROUPS)], axis=1) * inv
    gated = total * (gate * lax.logistic(gate))
    normed = []
    for g in range(GROUPS):
        part_g = gated[:, g * GW : g * GW + GW]
        mean = jnp.sum(part_g * part_g, axis=1, keepdims=True) / GW
        normed.append(part_g * lax.rsqrt(mean + eps))
    nrm[z] = (jnp.concatenate(normed, axis=1) * out_gain).astype(bf16)
    for d in (4, 3, 5, 2, 6, 1, 7):
        pltpu.make_async_remote_copy(
            nrm.at[z], nrm.at[z], ssem.at[8], rsem.at[8], **at(lax.rem(z + d, NZ), x, t)
        ).start()

    arrived(wor, 3, rsem.at[7])
    arrived(nrm, 7, rsem.at[8])
    rows64 = nrm[...].astype(f32).reshape(64, WIDTH).astype(bf16)
    for d in (2, 1, 3, 0):
        xp = lax.rem(x + d, NX)
        fs[d] = mm(rows64, wor[xp], 1, 1).astype(bf16)
        if d == 0:
            fr[x * NT + t] = fs[0]
        else:
            pltpu.make_async_remote_copy(
                fs.at[d], fr.at[x * NT + t], ssem.at[9], rsem.at[9], **at(z, xp, t)
            ).start()
        pltpu.make_async_remote_copy(
            fs.at[d], fr.at[x * NT + t], ssem.at[9], rsem.at[9], **at(z, xp, 1 - t)
        ).start()
    arrived(fr, 7, rsem.at[9])
    done = fr[...].astype(f32).reshape(NX, NT, 64, 64)
    done = (done[:, 0] + done[:, 1]).reshape(NX, NZ, ROWS, 64)
    done = jnp.stack([done[:, n] for n in range(NZ)], axis=0)
    mixed_o[...] = done.reshape(64, PROPS, 64).astype(bf16)

    arrived(tt, 3, ssem.at[0])
    arrived(wb, 3, ssem.at[1])
    arrived(wxr, 3, ssem.at[2])
    arrived(wgr, 3, ssem.at[3])
    arrived(s0, PEERS - 1, ssem.at[4])
    arrived(s1, PEERS - 1, ssem.at[5])
    arrived(s2, PEERS - 1, ssem.at[6])
    arrived(wor, 3, ssem.at[7])
    arrived(nrm, 7, ssem.at[8])
    arrived(fr, 7, ssem.at[9])
    state_out.wait()


def local(
    tokens, input_norm_gain, head_input_weight, output_gate_weight, state_maps_weight,
    step_size_weight, step_size_bias, head_decay_speed, proposal_decay_total, head_input_kernel,
    state_maps_kernel, head_direct_gain, grouped_norm_gain, output_weight, prior_state_value,
    previous_head_input, previous_input_maps, previous_log_decays, prior_heads_window,
    prior_maps_window, accepted,
):
    anywhere = pl.BlockSpec(memory_space=pl.ANY)
    vmem = pl.BlockSpec(memory_space=pltpu.VMEM)
    V, DMA = pltpu.VMEM, pltpu.SemaphoreType.DMA
    outs = (
        jax.ShapeDtypeStruct((64, PROPS, 64), bf16),
        jax.ShapeDtypeStruct((SEQS, HEADS, HEAD_DIM, STATE), f32),
        jax.ShapeDtypeStruct((SEQS, PROPS, WIDTH), bf16),
        jax.ShapeDtypeStruct((SEQS, PROPS, BC), bf16),
        jax.ShapeDtypeStruct((SEQS, PROPS, HEADS), f32),
        jax.ShapeDtypeStruct((7, SEQS, WIDTH), bf16),
        jax.ShapeDtypeStruct((SEQS, 7, 2, BC), bf16),
    )
    mixed, state, chi, cim, cld, chw, cmw = pl.pallas_call(
        kernel,
        out_shape=outs,
        in_specs=[anywhere] * 20 + [pl.BlockSpec(memory_space=pltpu.SMEM)],
        out_specs=[vmem, anywhere, vmem, vmem, vmem, vmem, vmem],
        scratch_shapes=[
            V((64, PROPS, 64), bf16), V((D,), bf16), V((64, WIDTH), bf16), V((64, WIDTH), bf16),
            V((64, 2, BC), bf16), V((48,), f32), V((48,), f32), V((SEQS, PROPS, HEADS), f32),
            V((4, WIDTH), bf16), V((4, 2, BC), bf16), V((48,), f32), V((2 * WIDTH,), bf16),
            V((64, WIDTH), bf16), V((SEQS, HEADS, HEAD_DIM, STATE), f32),
            V((SEQS, PROPS, WIDTH), bf16), V((SEQS, PROPS, BC), bf16),
            V((SEQS, PROPS, HEADS), f32), V((7, SEQS, WIDTH), bf16), V((SEQS, 7, 2, BC), bf16),
            V((128, 256), bf16), V((NX, 64, 256), bf16), V((NX, 64, 256), bf16),
            V((NX, 64, 256), bf16), V((NX, 64, GW), bf16), V((NX, 64, GW), bf16),
            V((PEERS, ROWS, GW), bf16), V((PEERS, ROWS, GW), bf16), V((PEERS, ROWS, GW), bf16),
            V((PEERS, ROWS, GW), bf16), V((PEERS, ROWS, GW), bf16), V((PEERS, ROWS, GW), bf16),
            V((NX, 64, WIDTH), bf16), V((SEQS, GROUPS, GW, STATE), bf16),
            V((NZ, ROWS, WIDTH), bf16), V((NX, 64, 64), bf16), V((NX * NT, 64, 64), bf16),
            DMA((20,)), DMA((10,)), DMA((10,)), DMA((1,)),
        ],
        compiler_params=pltpu.CompilerParams(
            collective_id=0, has_side_effects=True, vmem_limit_bytes=40 * 1024 * 1024
        ),
    )(
        tokens, input_norm_gain, head_input_weight, output_gate_weight, state_maps_weight,
        step_size_weight.T, step_size_bias, head_decay_speed, proposal_decay_total,
        head_input_kernel, state_maps_kernel, head_direct_gain, grouped_norm_gain,
        output_weight.T, prior_state_value, previous_head_input, previous_input_maps,
        previous_log_decays, jnp.transpose(prior_heads_window, (1, 0, 2)), prior_maps_window,
        accepted,
    )
    return mixed, state, chi, cim, cld, jnp.transpose(chw, (1, 0, 2)), cmw


def solution(mesh):
    seq = ("dp", "kv")
    return jax.shard_map(
        local,
        mesh=mesh,
        in_specs=(
            P("dp", None, "kv"), P(), P("kv", "tp"), P("kv", "tp"), P("kv", None, "tp"), P(), P(),
            P(), P(seq, None, "tp"), P(), P(), P(), P(), P("tp", "kv"), P(seq, "tp", None, None),
            P(seq, None, "tp"), P(seq, None, "tp"), P(seq, None, "tp"), P(seq, None, "tp"),
            P(seq, None, None, "tp"), P(seq),
        ),
        out_specs=(
            P("dp", None, "kv"), P(seq, "tp", None, None), P(seq, None, "tp"), P(seq, None, "tp"),
            P(seq, None, "tp"), P(seq, None, "tp"), P(seq, None, None, "tp"),
        ),
        check_vma=False,
    )
```

time: 151 us -> 68.3 us (0.45)
  waiting for transfers between devices: 58.7 us -> 0 us
  Pallas kernels: 0 us -> 45.4 us
  starting transfers between devices: 43.5 us -> 0 us
  other arithmetic: 13 us -> 0 us
  matrix products: 10.2 us -> 0 us
  blocking collectives: 8.91 us -> 0 us
  local copies, waits for them, and re-layouts: 14.5 us -> 21.4 us
    all_to_all x6 -> x0, waiting for transfers between devices: 58.7 us -> none  [the longest x4 34.7 us: summed_on_arrival(): lax.all_to_all(parts, axis, split_axis=0, concat_axis=0, tiled=True)]
    pallas_call x0 -> x1, Pallas kernels: none -> 45.4 us  [local(): pl.pallas_call(kernel, out_shape=outs, in_specs=[anywhere] * 20 + [pl.Blo...]
    all_to_all x6 -> x0, starting transfers between devices: 43.5 us -> none  [the longest x4 28.9 us: summed_on_arrival(): lax.all_to_all(parts, axis, split_axis=0, concat_axis=0, tiled=True)]
    unnamed x65 -> x49, local copies, waits for them, and re-layouts: 3.06 us -> 21.4 us
    dot_general x10 -> x0, matrix products: 10.2 us -> none  [the longest x1 2.54 us: local_mixer_output(): jnp.einsum('sthn,shpn->sthp', c_heads, carried, precision=lax.Precision.H...]
    all_to_all x1 -> x0, blocking collectives: 8.91 us -> none  [sent_to_all(): lax.all_to_all(jnp.broadcast_to(array[None], (devices, *array.shape)), ax...]
    add x2 -> x0, other arithmetic: 4.7 us -> none  [the longest x1 3.97 us: local_mixer_output(): carried * factor[:, :, None, None] + keep[:, :, None, None] * update]
    convert_element_type x11 -> x0, other arithmetic: 3.83 us -> none  [the longest x1 0.81 us: local(): gain_part.astype(jnp.float32)]
  transfers between devices with their start and end apart: 6 -> 0, of which waited for: 6 -> 0; matrix products, arithmetic and copies ran while one was open for 19% -> 0% of each run, Pallas kernels for 0% -> 0%
where the time goes in v1:
time: 68.3 us; the launch traced here: 67.5 us
  Pallas kernels  45.4 us (66%)
  local copies, waits for them, and re-layouts  21.4 us (31%)
    pallas_call x1, Pallas kernels, local(): pl.pallas_call(kernel, out_shape=outs, in_specs=[anywhere] * 20 + [pl.Blo...  45.4 us
    unnamed x49, local copies, waits for them, and re-layouts  21.4 us

profile of v1, /device:TPU:1, one launch (start us, length us, event | category | flops | bytes accessed | tf_op | source)
XLA Modules:
  0.0 67.5 jit_solution(11675579245982141470)
XLA Ops:
  0.6 0.0 copy-start
  0.7 1.4 %copy-done = f32[2,24,64,128]{3,2,1,0:T(8,128)S(1)} copy-done((f32[2,24,64,128]{3,2,1,0:T(8,128)S(1)}, f32[2,24,64,128]{3,2,1,0:T(8,128)}, u32[]{:S(2)}) %copy-start) | copy-done | bytes 1572888
  2.1 0.0 copy-start.1
  2.1 0.9 %copy-done.1 = bf16[64,1536]{1,0:T(8,128)(2,1)S(1)} copy-done((bf16[64,1536]{1,0:T(8,128)(2,1)S(1)}, bf16[64,1536]{1,0:T(8,128)(2,1)}, u32[]{:S(2)}) %copy-start.1) | copy-done | bytes 196632
  3.0 0.0 copy-start.2
  3.0 0.9 %copy-done.2 = bf16[64,1536]{1,0:T(8,128)(2,1)S(1)} copy-done((bf16[64,1536]{1,0:T(8,128)(2,1)S(1)}, bf16[64,1536]{1,0:T(8,128)(2,1)}, u32[]{:S(2)}) %copy-start.2) | copy-done | bytes 196632
  3.9 0.9 %copy-done.3 = bf16[2048,48]{0,1:T(8,128)(2,1)S(1)} copy-done((bf16[2048,48]{0,1:T(8,128)(2,1)S(1)}, bf16[2048,48]{0,1:T(8,128)(2,1)}, u32[]{:S(2)}) %copy-start.3) | copy-done | bytes 196632
  4.8 0.9 %copy-done.4 = bf16[1536,64]{0,1:T(8,128)(2,1)S(1)} copy-done((bf16[1536,64]{0,1:T(8,128)(2,1)S(1)}, bf16[1536,64]{0,1:T(8,128)(2,1)}, u32[]{:S(2)}) %copy-start.4) | copy-done | bytes 196632
  5.8 0.9 %copy-done.5 = bf16[64,2,512]{2,1,0:T(2,128)(2,1)S(1)} copy-done((bf16[64,2,512]{2,1,0:T(2,128)(2,1)S(1)}, bf16[64,2,512]{2,1,0:T(2,128)(2,1)}, u32[]{:S(2)}) %copy-start.5) | copy-done | bytes 131096
  6.7 0.8 %copy-done.6 = bf16[64,4,64]{2,1,0:T(4,128)(2,1)S(1)} copy-done((bf16[64,4,64]{2,1,0:T(4,128)(2,1)S(1)}, bf16[64,4,64]{2,1,0:T(4,128)(2,1)}, u32[]{:S(2)}) %copy-start.6) | copy-done | bytes 32792
  7.5 0.8 %copy-done.7 = bf16[2,7,1536]{2,0,1:T(2,128)(2,1)S(1)} copy-done((bf16[2,7,1536]{2,0,1:T(2,128)(2,1)S(1)}, bf16[2,7,1536]{2,0,1:T(2,128)(2,1)}, u32[]{:S(2)}) %copy-start.7) | copy-done | bytes 43032
  8.3 0.7 %copy-done.8 = bf16[2,7,2,512]{3,2,1,0:T(2,128)(2,1)S(1)} copy-done((bf16[2,7,2,512]{3,2,1,0:T(2,128)(2,1)S(1)}, bf16[2,7,2,512]{3,2,1,0:T(2,128)(2,1)}, u32[]{:S(2)}) %copy-start.8) | copy-done | bytes 28696
  9.0 0.7 %copy-done.9 = bf16[4,3072]{1,0:T(4,128)(2,1)S(1)} copy-done((bf16[4,3072]{1,0:T(4,128)(2,1)S(1)}, bf16[4,3072]{1,0:T(4,128)(2,1)}, u32[]{:S(2)}) %copy-start.9) | copy-done | bytes 24600
  9.8 0.7 %copy-done.10 = bf16[2,4,1536]{2,1,0:T(4,128)(2,1)S(1)} copy-done((bf16[2,4,1536]{2,1,0:T(4,128)(2,1)S(1)}, bf16[2,4,1536]{2,1,0:T(4,128)(2,1)}, u32[]{:S(2)}) %copy-start.10) | copy-done | bytes 24600
  10.5 0.7 %copy-done.11 = bf16[4,2,1024]{2,1,0:T(2,128)(2,1)S(1)} copy-done((bf16[4,2,1024]{2,1,0:T(2,128)(2,1)S(1)}, bf16[4,2,1024]{2,1,0:T(2,128)(2,1)}, u32[]{:S(2)}) %copy-start.11) | copy-done | bytes 16408
  11.2 0.7 %copy-done.12 = bf16[2,4,512]{2,1,0:T(4,128)(2,1)S(1)} copy-done((bf16[2,4,512]{2,1,0:T(4,128)(2,1)S(1)}, bf16[2,4,512]{2,1,0:T(4,128)(2,1)}, u32[]{:S(2)}) %copy-start.12) | copy-done | bytes 8216
  11.9 0.7 %copy-done.13 = bf16[3072]{0:T(1024)(128)(2,1)S(1)} copy-done((bf16[3072]{0:T(1024)(128)(2,1)S(1)}, bf16[3072]{0:T(1024)(128)(2,1)}, u32[]{:S(2)}) %copy-start.13) | copy-done | bytes 6168
  12.6 0.7 %copy-done.14 = bf16[2048]{0:T(1024)(128)(2,1)S(1)} copy-done((bf16[2048]{0:T(1024)(128)(2,1)S(1)}, bf16[2048]{0:T(1024)(128)(2,1)}, u32[]{:S(2)}) %copy-start.14) | copy-done | bytes 4120
  13.3 0.7 %copy-done.15 = f32[2,4,24]{2,1,0:T(4,128)S(1)} copy-done((f32[2,4,24]{2,1,0:T(4,128)S(1)}, f32[2,4,24]{2,1,0:T(4,128)}, u32[]{:S(2)}) %copy-start.15) | copy-done | bytes 792
  14.0 0.7 %copy-done.16 = f32[2,4,24]{2,1,0:T(4,128)S(1)} copy-done((f32[2,4,24]{2,1,0:T(4,128)S(1)}, f32[2,4,24]{2,1,0:T(4,128)}, u32[]{:S(2)}) %copy-start.16) | copy-done | bytes 792
  14.7 0.7 copy-done.17
  15.3 0.7 copy-done.18
  16.0 0.7 copy-done.19
  16.7 0.7 copy-done.20
  17.3 45.4 %shard_map.252 = (bf16[64,4,64]{2,1,0:T(4,128)(2,1)S(1)}, f32[2,24,64,128]{3,2,1,0:T(8,128)S(1)}, bf16[2,4,1536]{2,1,0:T(4,128)(2,1)S(1)}, bf16[2,4,512]{2,1,0:T...) custom-call(bf16[64,4,64]{2,1,0:T(4,128)(2,1)S(1)} %copy-done.6, ...), custom_call_target="tpu_custom_call" | custom-call | tf_op jit(solution)/shard_map/pallas_call | solution.py:393
  62.7 0.6 copy.35
  63.4 1.1 %copy.36 = f32[2,24,64,128]{3,2,1,0:T(8,128)} copy(f32[2,24,64,128]{3,2,1,0:T(8,128)S(1)} %get-tuple-element.29) | data formatting | bytes 3145728
  64.5 0.6 copy.37
  65.1 0.6 copy.38
  65.7 0.6 copy.39
  66.3 0.6 copy.40
  66.9 0.6 copy.41
  (18 shorter events, 0.0 us)
Async XLA Ops:
  0.6 1.4 %copy-start = (f32[2,24,64,128]{3,2,1,0:T(8,128)S(1)}, f32[2,24,64,128]{3,2,1,0:T(8,128)}, u32[]{:S(2)}) copy-start(f32[2,24,64,128]{3,2,1,0:T(8,128)} %psv_h.1) | copy-start | bytes 4718596
  2.1 0.9 %copy-start.1 = (bf16[64,1536]{1,0:T(8,128)(2,1)S(1)}, bf16[64,1536]{1,0:T(8,128)(2,1)}, u32[]{:S(2)}) copy-start(bf16[64,1536]{1,0:T(8,128)(2,1)} %wx_h.1) | copy-start | bytes 589828
  3.0 0.9 %copy-start.2 = (bf16[64,1536]{1,0:T(8,128)(2,1)S(1)}, bf16[64,1536]{1,0:T(8,128)(2,1)}, u32[]{:S(2)}) copy-start(bf16[64,1536]{1,0:T(8,128)(2,1)} %wg_h.1) | copy-start | bytes 589828
  3.9 0.9 %copy-start.3 = (bf16[2048,48]{0,1:T(8,128)(2,1)S(1)}, bf16[2048,48]{0,1:T(8,128)(2,1)}, u32[]{:S(2)}) copy-start(bf16[2048,48]{0,1:T(8,128)(2,1)} %param.26) | copy-start | bytes 589828
  4.8 0.9 %copy-start.4 = (bf16[1536,64]{0,1:T(8,128)(2,1)S(1)}, bf16[1536,64]{0,1:T(8,128)(2,1)}, u32[]{:S(2)}) copy-start(bf16[1536,64]{0,1:T(8,128)(2,1)} %param.34) | copy-start | bytes 589828
  5.8 0.9 %copy-start.5 = (bf16[64,2,512]{2,1,0:T(2,128)(2,1)S(1)}, bf16[64,2,512]{2,1,0:T(2,128)(2,1)}, u32[]{:S(2)}) copy-start(bf16[64,2,512]{2,1,0:T(2,128)(2,1)} %smw_h.1) | copy-start | bytes 393220
  6.7 0.8 %copy-start.6 = (bf16[64,4,64]{2,1,0:T(4,128)(2,1)S(1)}, bf16[64,4,64]{2,1,0:T(4,128)(2,1)}, u32[]{:S(2)}) copy-start(bf16[64,4,64]{2,1,0:T(4,128)(2,1)} %tok_h.1) | copy-start | bytes 98308
  7.5 0.8 %copy-start.7 = (bf16[2,7,1536]{2,0,1:T(2,128)(2,1)S(1)}, bf16[2,7,1536]{2,0,1:T(2,128)(2,1)}, u32[]{:S(2)}) copy-start(bf16[2,7,1536]{2,0,1:T(2,128)(2,1)} %param.39) | copy-start | bytes 129028
  8.3 0.7 %copy-start.8 = (bf16[2,7,2,512]{3,2,1,0:T(2,128)(2,1)S(1)}, bf16[2,7,2,512]{3,2,1,0:T(2,128)(2,1)}, u32[]{:S(2)}) copy-start(bf16[2,7,2,512]{3,2,1,0:T(2,128)(2,1)} %pmw_h.1) | copy-start | bytes 86020
  9.0 0.7 %copy-start.9 = (bf16[4,3072]{1,0:T(4,128)(2,1)S(1)}, bf16[4,3072]{1,0:T(4,128)(2,1)}, u32[]{:S(2)}) copy-start(bf16[4,3072]{1,0:T(4,128)(2,1)} %hik_h.1) | copy-start | bytes 73732
  9.8 0.7 %copy-start.10 = (bf16[2,4,1536]{2,1,0:T(4,128)(2,1)S(1)}, bf16[2,4,1536]{2,1,0:T(4,128)(2,1)}, u32[]{:S(2)}) copy-start(bf16[2,4,1536]{2,1,0:T(4,128)(2,1)} %phi_h.1) | copy-start | bytes 73732
  10.5 0.7 %copy-start.11 = (bf16[4,2,1024]{2,1,0:T(2,128)(2,1)S(1)}, bf16[4,2,1024]{2,1,0:T(2,128)(2,1)}, u32[]{:S(2)}) copy-start(bf16[4,2,1024]{2,1,0:T(2,128)(2,1)} %smk_h.1) | copy-start | bytes 49156
  11.2 0.7 %copy-start.12 = (bf16[2,4,512]{2,1,0:T(4,128)(2,1)S(1)}, bf16[2,4,512]{2,1,0:T(4,128)(2,1)}, u32[]{:S(2)}) copy-start(bf16[2,4,512]{2,1,0:T(4,128)(2,1)} %pim_h.1) | copy-start | bytes 24580
  11.9 0.7 %copy-start.13 = (bf16[3072]{0:T(1024)(128)(2,1)S(1)}, bf16[3072]{0:T(1024)(128)(2,1)}, u32[]{:S(2)}) copy-start(bf16[3072]{0:T(1024)(128)(2,1)} %gng_h.1) | copy-start | bytes 18436
  12.6 0.7 %copy-start.14 = (bf16[2048]{0:T(1024)(128)(2,1)S(1)}, bf16[2048]{0:T(1024)(128)(2,1)}, u32[]{:S(2)}) copy-start(bf16[2048]{0:T(1024)(128)(2,1)} %gain_h.1) | copy-start | bytes 12292
  13.3 0.7 %copy-start.15 = (f32[2,4,24]{2,1,0:T(4,128)S(1)}, f32[2,4,24]{2,1,0:T(4,128)}, u32[]{:S(2)}) copy-start(f32[2,4,24]{2,1,0:T(4,128)} %pdt_h.1) | copy-start | bytes 2308
  14.0 0.7 %copy-start.16 = (f32[2,4,24]{2,1,0:T(4,128)S(1)}, f32[2,4,24]{2,1,0:T(4,128)}, u32[]{:S(2)}) copy-start(f32[2,4,24]{2,1,0:T(4,128)} %pld_h.1) | copy-start | bytes 2308
  14.7 0.7 copy-start.17
  15.3 0.7 copy-start.18
  16.0 0.7 copy-start.19
  16.6 0.7 copy-start.20

commit v2 on v1

--- a/solution.py
+++ b/solution.py
@@ -66,11 +66,11 @@
 
 def kernel(
     tok_h, gain_h, wx_h, wg_h, smw_h, sw_h, ssb_h, hds_h, pdt_h, hik_h, smk_h, hdg_h, gng_h, wo_h,
-    psv_h, phi_h, pim_h, pld_h, phw_h, pmw_h, acc_s,
-    mixed_o, state_o, chi_o, cim_o, cld_o, chw_o, cmw_o,
+    psv_h, phi_h, pim_h, pld_h, phw_h, pmw_h, acc_h,
+    fr, state_o, chi_o, cim_o, cld_o, chw_o, cmw_o,
     tok, gain, wx, wg, smw, ssb, hds, pdt, hik, smk, hdg, gng, wo, psv, phi, pim, pld, phw, pmw,
-    sw, bcs, tt, wb, wxr, wgr, s0, s1, s2, r0, r1, r2, wor, sb, nrm, fs, fr,
-    lsem, ssem, rsem, osem,
+    sw, bcs, tt, wb, wxr, wgr, s0, s1, s2, r0, r1, r2, wor, sb, nrm, fs,
+    chi, cim, cld, chw, cmw, acc_s, lsem, ssem, rsem, osem,
 ):
     y, kv, t = lax.axis_index("dp"), lax.axis_index("kv"), lax.axis_index("tp")
     z, x = kv // NX, kv % NX
@@ -86,7 +86,7 @@
         (hik_h.at[:, pl.ds(pl.multiple_of(t * WIDTH, 128), WIDTH)], hik),
         (smk_h.at[:, :, pl.ds(pl.multiple_of(t * BC, 128), BC)], smk),
         (hdg_h, hdg), (gng_h, gng), (wo_h, wo), (phi_h, phi), (pim_h, pim), (pld_h, pld),
-        (phw_h, phw), (pmw_h, pmw), (psv_h, psv),
+        (phw_h, phw), (pmw_h, pmw), (psv_h, psv), (acc_h, acc_s),
     )
     for n, (src, dst) in enumerate(plan):
         loads[n] = pltpu.make_async_copy(src, dst, lsem.at[n])
@@ -195,6 +195,7 @@
             wo, wor.at[x], ssem.at[7], rsem.at[7], **at(z, lax.rem(x + d, NX), t)
         ).start()
 
+    loads[20].wait()
     acc = (acc_s[0], acc_s[1])
     row = iota((ROWS, 1), 0)
     acc_row = jnp.where(row < PROPS, acc[0], acc[1])
@@ -229,8 +230,13 @@
             )
             psv[b, g * PER : g * PER + PER] = new
             sb[b, g] = new.reshape(GW, STATE).astype(bf16)
-    state_out = pltpu.make_async_copy(psv, state_o, osem.at[0])
-    state_out.start()
+    outs = []
+
+    def put(n, src, dst):
+        outs.append(pltpu.make_async_copy(src, dst, osem.at[n]))
+        outs[-1].start()
+
+    put(0, psv, state_o)
 
     pick_x, pick_bc = heads_selection(acc), maps_selection(acc)
     for n in (6, 7, 8, 9, 10, 11, 12, 17, 18):
@@ -262,7 +268,8 @@
     raw_b = jnp.concatenate([sum0[g, :, 0:128] for g in range(GROUPS)], axis=1) * inv
     raw_c = jnp.concatenate([sum0[g, :, 128:256] for g in range(GROUPS)], axis=1) * inv
     win_bc = mm(pick_bc, jnp.concatenate([old_bc, raw_b, raw_c], axis=0).astype(bf16))
-    cmw_v = win_bc[64:92].reshape(SEQS, 7, 2, BC).astype(bf16)
+    cmw[...] = win_bc[64:92].reshape(SEQS, 7, 2, BC).astype(bf16)
+    put(1, cmw, cmw_o)
     b_conv = taps_bc[0:1] * win_bc[0:8]
     c_conv = taps_bc[1:2] * win_bc[8:16]
     for k in range(1, 4):
@@ -281,9 +288,10 @@
         precision=HI,
     )
     cum_w, step_w, direct_w = wide[0:8], wide[8:16], wide[16:24]
-    cim_o[...] = b_conv.reshape(SEQS, PROPS, BC).astype(bf16)
-    cld_o[...] = decays.reshape(SEQS, PROPS, HEADS)
-    cmw_o[...] = cmw_v
+    cim[...] = b_conv.reshape(SEQS, PROPS, BC).astype(bf16)
+    put(2, cim, cim_o)
+    cld[...] = decays.reshape(SEQS, PROPS, HEADS)
+    put(3, cld, cld_o)
     from_state, pairs = [], []
     for g in range(GROUPS):
         lanes = slice(g * STATE, g * STATE + STATE)
@@ -298,13 +306,15 @@
     sum1 = jnp.sum(r1[...].astype(f32).reshape(NX, NZ, ROWS, GW), axis=1)
     raw_x = jnp.concatenate([sum1[g] for g in range(GROUPS)], axis=1) * inv
     win_x = mm(pick_x, jnp.concatenate([old_x, raw_x], axis=0).astype(bf16))
-    chw_o[...] = win_x[32:46].reshape(7, SEQS, WIDTH).astype(bf16)
+    chw[...] = win_x[32:46].reshape(7, SEQS, WIDTH).astype(bf16)
+    put(4, chw, chw_o)
     x_conv = taps_x[0:1] * win_x[0:8]
     for k in range(1, 4):
         x_conv = x_conv + taps_x[k : k + 1] * win_x[8 * k : 8 * k + 8]
     x_conv = x_conv * lax.logistic(x_conv)
     weighted = step_w * x_conv
-    chi_o[...] = weighted.reshape(SEQS, PROPS, WIDTH).astype(bf16)
+    chi[...] = weighted.reshape(SEQS, PROPS, WIDTH).astype(bf16)
+    put(5, chi, chi_o)
     total = from_state + direct_w * x_conv
     for d in range(PROPS):
         score = [
@@ -344,7 +354,7 @@
         xp = lax.rem(x + d, NX)
         fs[d] = mm(rows64, wor[xp], 1, 1).astype(bf16)
         if d == 0:
-            fr[x * NT + t] = fs[0]
+            put(6, fs.at[0], fr.at[x * NT + t])
         else:
             pltpu.make_async_remote_copy(
                 fs.at[d], fr.at[x * NT + t], ssem.at[9], rsem.at[9], **at(z, xp, t)
@@ -353,10 +363,6 @@
             fs.at[d], fr.at[x * NT + t], ssem.at[9], rsem.at[9], **at(z, xp, 1 - t)
         ).start()
     arrived(fr, 7, rsem.at[9])
-    done = fr[...].astype(f32).reshape(NX, NT, 64, 64)
-    done = (done[:, 0] + done[:, 1]).reshape(NX, NZ, ROWS, 64)
-    done = jnp.stack([done[:, n] for n in range(NZ)], axis=0)
-    mixed_o[...] = done.reshape(64, PROPS, 64).astype(bf16)
 
     arrived(tt, 3, ssem.at[0])
     arrived(wb, 3, ssem.at[1])
@@ -368,7 +374,32 @@
     arrived(wor, 3, ssem.at[7])
     arrived(nrm, 7, ssem.at[8])
     arrived(fr, 7, ssem.at[9])
-    state_out.wait()
+    for copy in outs:
+        copy.wait()
+
+
+def finish(fr_h, *refs):
+    ins, outs, fr, mixed = refs[:6], refs[7:13], refs[13], refs[14]
+    mids, sems = refs[15:21], refs[21]
+    mixed_o = refs[6]
+    first = [pltpu.make_async_copy(fr_h, fr, sems.at[0])]
+    first += [pltpu.make_async_copy(a, b, sems.at[n + 1]) for n, (a, b) in enumerate(zip(ins, mids))]
+    for copy in first:
+        copy.start()
+    second = [pltpu.make_async_copy(a, b, sems.at[n + 7]) for n, (a, b) in enumerate(zip(mids, outs))]
+    first[0].wait()
+    done = fr[...].astype(f32).reshape(NX, NT, 64, 64)
+    done = (done[:, 0] + done[:, 1]).reshape(NX, NZ, ROWS, 64)
+    done = jnp.stack([done[:, n] for n in range(NZ)], axis=0)
+    mixed[...] = done.reshape(64, PROPS, 64).astype(bf16)
+    last = pltpu.make_async_copy(mixed, mixed_o, sems.at[13])
+    last.start()
+    for a, b in zip(first[1:], second):
+        a.wait()
+        b.start()
+    for copy in second:
+        copy.wait()
+    last.wait()
 
 
 def local(
@@ -379,10 +410,9 @@
     prior_maps_window, accepted,
 ):
     anywhere = pl.BlockSpec(memory_space=pl.ANY)
-    vmem = pl.BlockSpec(memory_space=pltpu.VMEM)
     V, DMA = pltpu.VMEM, pltpu.SemaphoreType.DMA
     outs = (
-        jax.ShapeDtypeStruct((64, PROPS, 64), bf16),
+        jax.ShapeDtypeStruct((NX * NT, 64, 64), bf16),
         jax.ShapeDtypeStruct((SEQS, HEADS, HEAD_DIM, STATE), f32),
         jax.ShapeDtypeStruct((SEQS, PROPS, WIDTH), bf16),
         jax.ShapeDtypeStruct((SEQS, PROPS, BC), bf16),
@@ -390,11 +420,11 @@
         jax.ShapeDtypeStruct((7, SEQS, WIDTH), bf16),
         jax.ShapeDtypeStruct((SEQS, 7, 2, BC), bf16),
     )
-    mixed, state, chi, cim, cld, chw, cmw = pl.pallas_call(
+    results = pl.pallas_call(
         kernel,
         out_shape=outs,
-        in_specs=[anywhere] * 20 + [pl.BlockSpec(memory_space=pltpu.SMEM)],
-        out_specs=[vmem, anywhere, vmem, vmem, vmem, vmem, vmem],
+        in_specs=[anywhere] * 21,
+        out_specs=[anywhere] * 7,
         scratch_shapes=[
             V((64, PROPS, 64), bf16), V((D,), bf16), V((64, WIDTH), bf16), V((64, WIDTH), bf16),
             V((64, 2, BC), bf16), V((48,), f32), V((48,), f32), V((SEQS, PROPS, HEADS), f32),
@@ -407,11 +437,13 @@
             V((PEERS, ROWS, GW), bf16), V((PEERS, ROWS, GW), bf16), V((PEERS, ROWS, GW), bf16),
             V((PEERS, ROWS, GW), bf16), V((PEERS, ROWS, GW), bf16), V((PEERS, ROWS, GW), bf16),
             V((NX, 64, WIDTH), bf16), V((SEQS, GROUPS, GW, STATE), bf16),
-            V((NZ, ROWS, WIDTH), bf16), V((NX, 64, 64), bf16), V((NX * NT, 64, 64), bf16),
-            DMA((20,)), DMA((10,)), DMA((10,)), DMA((1,)),
+            V((NZ, ROWS, WIDTH), bf16), V((NX, 64, 64), bf16),
+            V((SEQS, PROPS, WIDTH), bf16), V((SEQS, PROPS, BC), bf16),
+            V((SEQS, PROPS, HEADS), f32), V((7, SEQS, WIDTH), bf16), V((SEQS, 7, 2, BC), bf16),
+            pltpu.SMEM((SEQS,), i32), DMA((21,)), DMA((10,)), DMA((10,)), DMA((7,)),
         ],
         compiler_params=pltpu.CompilerParams(
-            collective_id=0, has_side_effects=True, vmem_limit_bytes=40 * 1024 * 1024
+            collective_id=0, has_side_effects=True, vmem_limit_bytes=60 * 1024 * 1024
         ),
     )(
         tokens, input_norm_gain, head_input_weight, output_gate_weight, state_maps_weight,
@@ -421,6 +453,17 @@
         previous_log_decays, jnp.transpose(prior_heads_window, (1, 0, 2)), prior_maps_window,
         accepted,
     )
+    finals = (jax.ShapeDtypeStruct((64, PROPS, 64), bf16), *outs[1:])
+    mixed, state, chi, cim, cld, chw, cmw = pl.pallas_call(
+        finish,
+        out_shape=finals,
+        in_specs=[anywhere] * 7,
+        out_specs=[anywhere] * 7,
+        scratch_shapes=[
+            V((NX * NT, 64, 64), bf16), V((64, PROPS, 64), bf16),
+            *(V(o.shape, o.dtype) for o in outs[1:]), DMA((14,)),
+        ],
+    )(*results)
     return mixed, state, chi, cim, cld, jnp.transpose(chw, (1, 0, 2)), cmw
 
 

time: 68.3 us -> 47 us (0.69)
  local copies, waits for them, and re-layouts: 21.4 us -> 0 us
  Pallas kernels: 45.4 us -> 46.2 us
    unnamed x49 -> x0, local copies, waits for them, and re-layouts: 21.4 us -> none
    pallas_call x1 -> x2, Pallas kernels: 45.4 us -> 46.2 us  [the longest x1 43.5 us: local(): pl.pallas_call(kernel, out_shape=outs, in_specs=[anywhere] * 21, out_spec...]
where the time goes in v2:
time: 47 us; the launch traced here: 46.9 us
  Pallas kernels  46.2 us (98%)
  between operations  0.65 us (1%)
    pallas_call x1, Pallas kernels, local(): pl.pallas_call(kernel, out_shape=outs, in_specs=[anywhere] * 21, out_spec...  43.5 us
    pallas_call x1, Pallas kernels, local(): pl.pallas_call(finish, out_shape=finals, in_specs=[anywhere] * 7, out_spe...  2.77 us

profile of v2, /device:TPU:1, one launch (start us, length us, event | category | flops | bytes accessed | tf_op | source)
XLA Modules:
  0.0 46.9 jit_solution(4035131909082490361)
XLA Ops:
  0.6 43.5 %shard_map.252 = (bf16[8,64,64]{2,1,0:T(8,128)(2,1)}, f32[2,24,64,128]{3,2,1,0:T(8,128)}, bf16[2,4,1536]{2,1,0:T(4,128)(2,1)}, bf16[2,4,512]{2,1,0:T(4,128)(2,1)...) custom-call(bf16[64,4,64]{2,1,0:T(4,128)(2,1)} %tok_h.1, ...), custom_call_target="tpu_custom_call" | custom-call | tf_op jit(solution)/shard_map/pallas_call | solution.py:423
  44.1 2.8 %shard_map.253 = (bf16[64,4,64]{2,1,0:T(4,128)(2,1)}, f32[2,24,64,128]{3,2,1,0:T(8,128)}, bf16[2,4,1536]{2,1,0:T(4,128)(2,1)}, bf16[2,4,512]{2,1,0:T(4,128)(2,1)...) custom-call(bf16[8,64,64]{2,1,0:T(8,128)(2,1)} %get-tuple-element.21.fr_h, ...), custom_call_target="tpu_custom_call" | custom-call | tf_op jit(solution)/shard_map/pallas_call | solution.py:457

commit v3 on v2

v3 whole, which is shorter than its diff:
```python
import functools

import jax
import jax.numpy as jnp
from jax import lax
from jax.experimental import pallas as pl
from jax.experimental.pallas import tpu as pltpu
from jax.sharding import PartitionSpec as P

MESH = pl.DeviceIdType.MESH
HI = lax.Precision.HIGHEST
f32, bf16, i32 = jnp.float32, jnp.bfloat16, jnp.int32

NX, NY, NZ, NT = 4, 4, 8, 2
PEERS = NX * NZ
D, STATE, HEAD_DIM = 2048, 128, 64
SEQS, PROPS, ROWS = 2, 4, 8
HEADS, GROUPS, PER = 24, 4, 6
WIDTH, GW = 1536, 384
BC = 512
eps = 1e-06


def iota(shape, dim):
    return lax.broadcasted_iota(i32, shape, dim)


def mm(a, b, ca=1, cb=0, precision=None):
    return lax.dot_general(
        a, b, (((ca,), (cb,)), ((), ())), precision=precision, preferred_element_type=f32
    )


def heads_selection(acc):
    shape = (48, 24)
    i, j = iota(shape, 0), iota(shape, 1)
    out = i >= 32
    b = jnp.where(out, i & 1, (i >> 2) & 1)
    pos = jnp.where(out, (i - 32) >> 1, (i & 3) + (i >> 3))
    acc_b = jnp.where(b == 0, acc[0], acc[1])
    old = (j < 14) & ((j & 1) == b) & ((j >> 1) == acc_b + pos)
    raw = (j >= 16) & (((j - 16) >> 2) == b) & (((j - 16) & 3) == pos - 3)
    pick = jnp.where(pos < 3, jnp.where(old, 1.0, 0.0), jnp.where(raw, 1.0, 0.0))
    return pick.astype(bf16)


def maps_selection(acc):
    shape = (96, 48)
    i, j = iota(shape, 0), iota(shape, 1)
    out = i >= 64
    o = i - 64
    ob = jnp.where(o >= 14, 1, 0)
    orem = o - 14 * ob
    b = jnp.where(out, ob, (i >> 2) & 1)
    pos = jnp.where(out, orem >> 1, (i & 3) + (i >> 4))
    kind = jnp.where(out, orem & 1, (i >> 3) & 1)
    acc_b = jnp.where(b == 0, acc[0], acc[1])
    jb = jnp.where(j >= 14, 1, 0)
    jrem = j - 14 * jb
    old = (j < 28) & (jb == b) & ((jrem & 1) == kind) & ((jrem >> 1) == acc_b + pos)
    jr = j - 32
    raw = (j >= 32) & ((jr >> 3) == kind) & (((jr >> 2) & 1) == b) & ((jr & 3) == pos - 3)
    pick = jnp.where(pos < 3, jnp.where(old, 1.0, 0.0), jnp.where(raw, 1.0, 0.0))
    return pick.astype(bf16)


def kernel(
    tok_h, gain_h, wx_h, wg_h, smw_h, sw_h, ssb_h, hds_h, pdt_h, hik_h, smk_h, hdg_h, gng_h, wo_h,
    psv_h, phi_h, pim_h, pld_h, phw_h, pmw_h, acc_h,
    fr, state_o, chi_o, cim_o, cld_o, chw_o, cmw_o,
    tok, gain, wxg, smw, ssb, hds, pdt, hik, smk, hdg, gng, wo, psv, phi, pim, pld, phw, pmw,
    sw, bcs, tt, lhs, wr, send, got, steps_out, steps_in, wor, sb, nrm, fs,
    chi, cim, cld, chw, cmw, acc_s, lsem, ssem, rsem, osem, level_sem,
):
    y, kv, t = lax.axis_index("dp"), lax.axis_index("kv"), lax.axis_index("tp")
    z, x = kv // NX, kv % NX
    pair, half = z // 2, z % 2

    def at(zz, xx, tt_):
        return dict(device_id=(y, zz * NX + xx, tt_), device_id_type=MESH)

    def over(d):
        return dict(device_id=(lax.rem(y + d, NY), kv, t), device_id_type=MESH)

    loads = {}
    plan = (
        (tok_h, tok), (gain_h, gain), (smw_h, smw), (wx_h, wxg.at[0]), (wg_h, wxg.at[1]),
        (sw_h.at[:, pl.ds(pl.multiple_of(pair * 512, 512), 512)], sw.at[pl.ds(0, 48)]),
        (ssb_h, ssb), (hds_h, hds), (pdt_h, pdt),
        (hik_h.at[:, pl.ds(pl.multiple_of(t * WIDTH, 128), WIDTH)], hik),
        (smk_h.at[:, :, pl.ds(pl.multiple_of(t * BC, 128), BC)], smk),
        (hdg_h, hdg), (gng_h, gng), (wo_h, wo), (phi_h, phi), (pim_h, pim), (pld_h, pld),
        (phw_h, phw), (pmw_h, pmw), (psv_h, psv), (acc_h, acc_s),
    )
    for n, (src, dst) in enumerate(plan):
        loads[n] = pltpu.make_async_copy(src, dst, lsem.at[n])
        loads[n].start()

    barrier = pltpu.get_barrier_semaphore()

    row_peers = [(0, 2), (0, 1), (0, 3)]
    up_peers = [(1, 2), (1, 1), (1, 3), (1, 0)]
    down_peers = [(NZ - 1, dx) for _, dx in up_peers]

    def near(dz, dx):
        return lax.rem(x + dx, NX), at(lax.rem(z + dz, NZ), lax.rem(x + dx, NX), t)

    for dz, dx in row_peers + up_peers + down_peers:
        pl.semaphore_signal(barrier, inc=1, **near(dz, dx)[1])
    for d in range(NX):
        pl.semaphore_signal(barrier, inc=1, **at(z, lax.rem(x + d, NX), 1 - t))
    for d in range(1, NY):
        pl.semaphore_signal(barrier, inc=1, **over(d))

    for n in (0, 1, 2):
        loads[n].wait()
    tok32 = tok[...].astype(f32).reshape(256, 64)
    gains = gain[...].astype(f32).reshape(16, 128)
    gain_row = jnp.sum(
        jnp.where(iota((16, 128), 0) == kv // 2, gains, 0.0), axis=0, keepdims=True
    )
    gain_row = jnp.where(kv % 2 == 0, gain_row[:, :64], gain_row[:, 64:])
    tt[x, 0:64] = (tok32 * gain_row).astype(bf16).T
    sumsq = jnp.sum(jnp.square(tok32.T), axis=0, keepdims=True)
    high = sumsq.astype(bf16).astype(f32)
    line = iota((16, 256), 0)
    tt[x, 64:80] = jnp.where(
        line == 0, high, jnp.where(line == 1, sumsq - high, 0.0)
    ).astype(bf16)
    for n in range(2):
        part = smw[:, n, :]
        for g in range(GROUPS):
            bcs[n * GROUPS + g] = part[:, g * STATE : g * STATE + STATE]
    sw[48:128] = jnp.zeros((80, 512), bf16)

    def columns(c, h, xx):
        if c == 0:
            return bcs.at[h * NX + xx]
        return wxg.at[
            h if c == 1 else 1 - h, :, pl.ds(pl.multiple_of(xx * GW + (c - 1) * 128, 128), 128)
        ]

    loads[3].wait()
    loads[4].wait()
    for c in range(4):
        wr[c, x] = columns(c, half, x)[...]

    pl.semaphore_wait(barrier, 11 + NX + NY - 1)

    lanes_t = pl.ds(pl.multiple_of(t * 128, 128), 128)
    for peers, base in ((up_peers, 8), (down_peers, 4), (row_peers, 0)):
        for dz, dx in peers:
            pltpu.make_async_remote_copy(
                tt.at[x, :, lanes_t],
                tt.at[base + x, :, lanes_t],
                ssem.at[4],
                rsem.at[4],
                **near(dz, dx)[1],
            ).start()
    for c in range(4):
        for peers, h, base in (
            (down_peers if c < 2 else up_peers, 1 - half, 4),
            (row_peers, half, 0),
        ):
            for dz, dx in peers:
                xx, to = near(dz, dx)
                pltpu.make_async_remote_copy(
                    columns(c, h, xx), wr.at[c, base + x], ssem.at[c], rsem.at[c], **to
                ).start()

    def pass_on(level):
        for n, dz in enumerate((1, NZ - 1)):
            pl.semaphore_signal(level_sem.at[level, n], inc=1, **near(dz, 0)[1])

    def hear(level):
        for n in range(2):
            pl.semaphore_wait(level_sem.at[level, n], 1)

    pass_on(0)

    def arrived(buffer, count, sem):
        block = buffer.at[pl.ds(0, count)]
        pltpu.make_async_copy(block, block, sem).wait()

    from_me = (x * 2 + half) * 4 + pair

    def spread(src, dst, index, n):
        def one(d, _):
            other = lax.rem(kv + d, PEERS)
            pltpu.make_async_remote_copy(
                src.at[other],
                dst.at[index],
                ssem.at[n],
                rsem.at[n],
                device_id=(y, other, t),
                device_id_type=MESH,
            ).start()
            return 0

        lax.fori_loop(1, PEERS, one, 0)
        dst[index] = src[kv]

    loads[20].wait()
    acc = (acc_s[0], acc_s[1])
    row = iota((ROWS, 1), 0)
    acc_row = jnp.where(row < PROPS, acc[0], acc[1])
    keep = jnp.where((row & 3) < acc_row, 1.0, 0.0)
    r8, c8 = iota((ROWS, ROWS), 0), iota((ROWS, ROWS), 1)
    same = (r8 >> 2) == (c8 >> 2)
    expand = jnp.where(iota((HEADS, WIDTH), 1) // HEAD_DIM == iota((HEADS, WIDTH), 0), 1.0, 0.0)
    for n in (14, 15, 16):
        loads[n].wait()
    kept = pld[...].reshape(ROWS, HEADS) * keep
    later = mm(jnp.where(same & (c8 > r8), 1.0, 0.0), kept, precision=HI)
    coef = mm(keep * jnp.exp(later), expand, precision=HI)
    scaled = coef * phi[...].astype(f32).reshape(ROWS, WIDTH)
    s_hi = scaled.astype(bf16)
    s_lo = (scaled - s_hi.astype(f32)).astype(bf16)
    updates = jnp.concatenate([s_hi.astype(f32), s_lo.astype(f32)], axis=0).astype(bf16)
    keys = pim[...].astype(f32).reshape(ROWS, BC)
    loads[19].wait()
    for b in range(SEQS):
        mine = (row >> 2) == b
        logs = mm(jnp.where(mine, kept, 0.0), jnp.ones((ROWS, STATE), f32), 0, 0, precision=HI)
        factor = jnp.exp(logs)
        keys_b = jnp.where(mine, keys, 0.0)
        keys_b = jnp.concatenate([keys_b, keys_b], axis=0).astype(bf16)
        for g in range(GROUPS):
            upd = mm(
                updates[:, g * GW : g * GW + GW], keys_b[:, g * STATE : g * STATE + STATE], 0, 0
            )
            new = (
                psv[b, g * PER : g * PER + PER] * factor[g * PER : g * PER + PER][:, None, :]
                + upd.reshape(PER, HEAD_DIM, STATE)
            )
            psv[b, g * PER : g * PER + PER] = new
            sb[b, g] = new.reshape(GW, STATE).astype(bf16)
    outs = []

    def put(n, src, dst):
        outs.append(pltpu.make_async_copy(src, dst, osem.at[n]))
        outs[-1].start()

    put(0, psv, state_o)

    for level in range(3):
        hear(level)
        if level < 2:
            pass_on(level + 1)

    loads[13].wait()
    wor[x] = wo[...]
    mine = pl.ds(pl.multiple_of(y * 16, 16), 16)
    quarters = wor.at[:, pl.ds(0, 16)]
    three_quarters = wor.at[:, pl.ds(0, 48)]

    steps_mine = (half == 0) & (x == pair)
    halves = tt.at[:, :, pl.ds(0, 128)]
    arrived(halves, 11, rsem.at[4])
    blocks = [tt.at[pl.ds(4, 8), :, lanes_t]]
    blocks += [tt.at[lax.rem(x + d, NX), :, lanes_t] for d in range(1, NX)]
    for block in blocks:
        pltpu.make_async_remote_copy(
            block, block, ssem.at[14], rsem.at[14], **at(z, x, 1 - t)
        ).start()
    arrived(halves, 11, rsem.at[14])
    lhs[...] = tt[:, 0:64].reshape(768, 256).T
    for c in range(4):
        if c == 0:
            loads[5].wait()
        arrived(wr.at[c], 7, rsem.at[c])
        if c < 2:
            part = mm(lhs[:, 0:512], wr[c].reshape(512, 128))
        else:
            part = mm(lhs[:, 0:256], wr[c, 0:4].reshape(256, 128))
            part = part + mm(lhs[:, 512:768], wr[c, 4:8].reshape(256, 128))
        send[c] = part.reshape(PEERS, ROWS, 128).astype(bf16)
        spread(send.at[c], got.at[c], from_me, 5 + c)
        if c == 1:
            for d in (2, 1, 3):
                pltpu.make_async_remote_copy(
                    wo.at[mine], wor.at[x, mine], ssem.at[10], rsem.at[10],
                    **at(z, lax.rem(x + d, NX), t),
                ).start()
        if c == 0:

            @pl.when(steps_mine)
            def _():
                steps = mm(lhs[:, 0:512], sw[...], 1, 1)
                squares = jnp.sum(tt[0:8, 64:80].astype(f32), axis=0)
                pick = jnp.where(
                    (iota((16, 128), 1) == 64) & (iota((16, 128), 0) < 2), 1.0, 0.0
                )
                squares = mm(squares, pick, 0, 0, precision=HI)
                total = squares[:, 64:65]
                high = total.astype(bf16).astype(f32)
                lane = iota((256, 128), 1)
                steps = jnp.where(lane == 64, high, jnp.where(lane == 65, total - high, steps))
                steps_out[...] = steps.reshape(PEERS, ROWS, 128).astype(bf16)
                spread(steps_out, steps_in, pair, 9)

    arrived(quarters, 3, rsem.at[10])
    for d in (2, 1, 3):
        for e in (2, 1, 3):
            block = wor.at[lax.rem(x + d, NX), mine]
            pltpu.make_async_remote_copy(
                block, block, ssem.at[13], rsem.at[13], **over(e)
            ).start()

    pick_x, pick_bc = heads_selection(acc), maps_selection(acc)
    for n in (6, 7, 8, 9, 10, 11, 12, 17, 18):
        loads[n].wait()
    old_x = phw[...].astype(f32).reshape(14, WIDTH)
    old_x = jnp.concatenate([old_x, jnp.zeros((2, WIDTH), f32)], axis=0)
    old_bc = pmw[...].astype(f32).reshape(28, BC)
    old_bc = jnp.concatenate([old_bc, jnp.zeros((4, BC), f32)], axis=0)
    taps_x = hik[...].astype(f32)
    taps_bc = smk[...].astype(f32).reshape(8, BC)

    def own_heads(ref):
        v = ref[...].reshape(1, 2 * HEADS)
        return jnp.where(t == 0, v[:, :HEADS], v[:, HEADS:])

    speed, direct, bias = own_heads(hds), own_heads(hdg), own_heads(ssb)
    gngv = gng[...].astype(f32).reshape(1, 2 * WIDTH)
    out_gain = jnp.where(t == 0, gngv[:, :WIDTH], gngv[:, WIDTH:])

    def total(c):
        return jnp.sum(got[c].astype(f32).reshape(NX, 2, 4, ROWS, 128), axis=2)

    arrived(got.at[0], PEERS - 1, rsem.at[5])

    @pl.when(steps_mine)
    def _():
        arrived(steps_in, 3, rsem.at[9])

    @pl.when(jnp.logical_not(steps_mine))
    def _():
        arrived(steps_in, 4, rsem.at[9])

    tail = jnp.sum(steps_in[...].astype(f32), axis=0)
    lane8 = iota((ROWS, 128), 1)
    squares = jnp.sum(jnp.where((lane8 == 64) | (lane8 == 65), tail, 0.0), axis=1, keepdims=True)
    inv = lax.rsqrt(squares / D + eps)
    sum0 = total(0)
    raw_b = jnp.concatenate([sum0[g, 0] for g in range(GROUPS)], axis=1) * inv
    raw_c = jnp.concatenate([sum0[g, 1] for g in range(GROUPS)], axis=1) * inv
    win_bc = mm(pick_bc, jnp.concatenate([old_bc, raw_b, raw_c], axis=0).astype(bf16))
    cmw[...] = win_bc[64:92].reshape(SEQS, 7, 2, BC).astype(bf16)
    put(1, cmw, cmw_o)
    b_conv = taps_bc[0:1] * win_bc[0:8]
    c_conv = taps_bc[1:2] * win_bc[8:16]
    for k in range(1, 4):
        b_conv = b_conv + taps_bc[2 * k : 2 * k + 1] * win_bc[16 * k : 16 * k + 8]
        c_conv = c_conv + taps_bc[2 * k + 1 : 2 * k + 2] * win_bc[16 * k + 8 : 16 * k + 16]
    b_conv = b_conv * lax.logistic(b_conv)
    c_conv = c_conv * lax.logistic(c_conv)
    step_pre = tail * inv
    step_pre = jnp.where(t == 0, step_pre[:, :HEADS], step_pre[:, HEADS : 2 * HEADS]) + bias
    step = jnp.maximum(step_pre, 0.0) + jnp.log1p(jnp.exp(-jnp.abs(step_pre)))
    decays = pdt[...].reshape(ROWS, HEADS) - speed * step
    cum = mm(jnp.where(same & (c8 <= r8), 1.0, 0.0), decays, precision=HI)
    wide = mm(
        jnp.concatenate([cum, step, jnp.broadcast_to(direct, (ROWS, HEADS))], axis=0),
        expand,
        precision=HI,
    )
    cim[...] = b_conv.reshape(SEQS, PROPS, BC).astype(bf16)
    put(2, cim, cim_o)
    cld[...] = decays.reshape(SEQS, PROPS, HEADS)
    put(3, cld, cld_o)
    from_state, pairs = [], []
    for g in range(GROUPS):
        lanes = slice(g * STATE, g * STATE + STATE)
        c_g = c_conv[:, lanes]
        y0 = mm(c_g.astype(bf16), sb[0, g], 1, 1)
        y1 = mm(c_g.astype(bf16), sb[1, g], 1, 1)
        from_state.append(jnp.where(row < PROPS, y0, y1))
        pairs.append(mm(c_g, b_conv[:, lanes], 1, 1, precision=HI))
    from_state = jnp.exp(wide[0:8]) * jnp.concatenate(from_state, axis=1)
    scores = []
    for d in range(PROPS):
        score = [
            jnp.broadcast_to(
                jnp.sum(jnp.where(c8 == r8 - d, p, 0.0), axis=1, keepdims=True), (ROWS, 128)
            )
            for p in pairs
        ]
        scores.append(jnp.concatenate(score, axis=1))

    def third(v, c):
        starts = [g * GW + (c - 1) * 128 for g in range(GROUPS)]
        return jnp.concatenate([v[:, n : n + 128] for n in starts], axis=1)

    def whole(thirds):
        return jnp.concatenate(
            [v[:, g * 128 : g * 128 + 128] for g in range(GROUPS) for v in thirds], axis=1
        )

    windows, inputs, gated = [], [], []
    for c in range(1, 4):
        wide_c, taps_c, old_c = third(wide, c), third(taps_x, c), third(old_x, c)
        cum_w, step_w, direct_w = wide_c[0:8], wide_c[8:16], wide_c[16:24]
        decay_w = [None]
        for d in range(1, PROPS):
            gap = jnp.where((row & 3) >= d, cum_w - pltpu.roll(cum_w, d, 0), 0.0)
            decay_w.append(jnp.exp(gap) * scores[d])
        arrived(got.at[c], PEERS - 1, rsem.at[5 + c])
        sum_c = total(c)
        heads_at = 0 if c == 1 else 1
        raw_x = jnp.concatenate([sum_c[g, heads_at] for g in range(GROUPS)], axis=1) * inv
        gate = jnp.concatenate([sum_c[g, 1 - heads_at] for g in range(GROUPS)], axis=1) * inv
        win_x = mm(pick_x, jnp.concatenate([old_c, raw_x], axis=0).astype(bf16))
        windows.append(win_x[32:46])
        x_conv = taps_c[0:1] * win_x[0:8]
        for k in range(1, 4):
            x_conv = x_conv + taps_c[k : k + 1] * win_x[8 * k : 8 * k + 8]
        x_conv = x_conv * lax.logistic(x_conv)
        weighted = step_w * x_conv
        inputs.append(weighted)
        heads = third(from_state, c) + direct_w * x_conv + scores[0] * weighted
        for d in range(1, PROPS):
            term = decay_w[d] * pltpu.roll(weighted, d, 0)
            heads = heads + jnp.where((row & 3) >= d, term, 0.0)
        gated.append(heads * (gate * lax.logistic(gate)))

    gated = whole(gated)
    normed = []
    for g in range(GROUPS):
        part_g = gated[:, g * GW : g * GW + GW]
        mean = jnp.sum(part_g * part_g, axis=1, keepdims=True) / GW
        normed.append(part_g * lax.rsqrt(mean + eps))
    nrm[z] = (jnp.concatenate(normed, axis=1) * out_gain).astype(bf16)
    for d in (4, 3, 5, 2, 6, 1, 7):
        pltpu.make_async_remote_copy(
            nrm.at[z], nrm.at[z], ssem.at[11], rsem.at[11], **at(lax.rem(z + d, NZ), x, t)
        ).start()
    chw[...] = whole(windows).reshape(7, SEQS, WIDTH).astype(bf16)
    put(4, chw, chw_o)
    chi[...] = whole(inputs).reshape(SEQS, PROPS, WIDTH).astype(bf16)
    put(5, chi, chi_o)

    arrived(three_quarters, 3, rsem.at[13])
    arrived(nrm, 7, rsem.at[11])
    rows64 = nrm[...].astype(f32).reshape(64, WIDTH).astype(bf16)
    for d in (2, 1, 3, 0):
        xp = lax.rem(x + d, NX)
        part = mm(rows64, wor[xp], 1, 1)
        fs[d] = jnp.concatenate([part[:32], part[32:]], axis=1).astype(bf16)
        if d == 0:
            put(6, fs.at[0], fr.at[x * NT + t])
        else:
            pltpu.make_async_remote_copy(
                fs.at[d], fr.at[x * NT + t], ssem.at[12], rsem.at[12], **at(z, xp, t)
            ).start()
        pltpu.make_async_remote_copy(
            fs.at[d], fr.at[x * NT + t], ssem.at[12], rsem.at[12], **at(z, xp, 1 - t)
        ).start()
    arrived(fr, 7, rsem.at[12])

    arrived(halves, 11, ssem.at[4])
    arrived(halves, 11, ssem.at[14])
    for c in range(4):
        arrived(wr.at[c], 7, ssem.at[c])
        arrived(send.at[c], PEERS - 1, ssem.at[5 + c])

    @pl.when(steps_mine)
    def _():
        arrived(steps_out, PEERS - 1, ssem.at[9])

    arrived(quarters, 3, ssem.at[10])
    arrived(three_quarters, 3, ssem.at[13])
    arrived(nrm, 7, ssem.at[11])
    arrived(fr, 7, ssem.at[12])
    for copy in outs:
        copy.wait()


def finish(fr_h, *refs):
    ins, outs, fr, mixed, mids, sems = (
        refs[:6], refs[7:13], refs[13], refs[14], refs[15:21], refs[21],
    )
    mixed_o = refs[6]

    def pieces(ref, n):
        if n > 0:
            return [ref]
        return [ref.at[b, pl.ds(h, 12)] for b in range(SEQS) for h in (0, 12)]

    trio = [
        piece
        for n in (1, 2, 3, 4, 5, 0)
        for piece in zip(pieces(ins[n], n), pieces(mids[n], n), pieces(outs[n], n))
    ]
    head = pltpu.make_async_copy(fr_h, fr, sems.at[0])
    head.start()
    first = [pltpu.make_async_copy(a, b, sems.at[1 + n]) for n, (a, b, _) in enumerate(trio)]
    second = [pltpu.make_async_copy(b, c, sems.at[10 + n]) for n, (_, b, c) in enumerate(trio)]
    for copy in first:
        copy.start()
    head.wait()
    done = fr[...].astype(f32).reshape(NX, NT, 32, 128)
    done = (done[:, 0] + done[:, 1]).reshape(NX, 4, ROWS, 128)
    done = jnp.stack(
        [done[:, n % 4, :, :64] if n < 4 else done[:, n % 4, :, 64:] for n in range(NZ)], axis=0
    )
    mixed[...] = done.reshape(64, PROPS, 64).astype(bf16)
    last = pltpu.make_async_copy(mixed, mixed_o, sems.at[19])
    last.start()
    for a, b in zip(first, second):
        a.wait()
        b.start()
    for copy in second:
        copy.wait()
    last.wait()


def local(
    tokens, input_norm_gain, head_input_weight, output_gate_weight, state_maps_weight,
    step_size_weight, step_size_bias, head_decay_speed, proposal_decay_total, head_input_kernel,
    state_maps_kernel, head_direct_gain, grouped_norm_gain, output_weight, prior_state_value,
    previous_head_input, previous_input_maps, previous_log_decays, prior_heads_window,
    prior_maps_window, accepted,
):
    anywhere = pl.BlockSpec(memory_space=pl.ANY)
    V, DMA = pltpu.VMEM, pltpu.SemaphoreType.DMA
    outs = (
        jax.ShapeDtypeStruct((NX * NT, 32, 128), bf16),
        jax.ShapeDtypeStruct((SEQS, HEADS, HEAD_DIM, STATE), f32),
        jax.ShapeDtypeStruct((SEQS, PROPS, WIDTH), bf16),
        jax.ShapeDtypeStruct((SEQS, PROPS, BC), bf16),
        jax.ShapeDtypeStruct((SEQS, PROPS, HEADS), f32),
        jax.ShapeDtypeStruct((7, SEQS, WIDTH), bf16),
        jax.ShapeDtypeStruct((SEQS, 7, 2, BC), bf16),
    )
    results = pl.pallas_call(
        kernel,
        out_shape=outs,
        in_specs=[anywhere] * 21,
        out_specs=[anywhere] * 7,
        scratch_shapes=[
            V((64, PROPS, 64), bf16), V((D,), bf16), V((2, 64, WIDTH), bf16),
            V((64, 2, BC), bf16), V((48,), f32), V((48,), f32), V((SEQS, PROPS, HEADS), f32),
            V((4, WIDTH), bf16), V((4, 2, BC), bf16), V((48,), f32), V((2 * WIDTH,), bf16),
            V((64, WIDTH), bf16), V((SEQS, HEADS, HEAD_DIM, STATE), f32),
            V((SEQS, PROPS, WIDTH), bf16), V((SEQS, PROPS, BC), bf16),
            V((SEQS, PROPS, HEADS), f32), V((7, SEQS, WIDTH), bf16), V((SEQS, 7, 2, BC), bf16),
            V((128, 512), bf16), V((8, 64, 128), bf16), V((12, 80, 256), bf16),
            V((256, 768), bf16), V((4, 8, 64, 128), bf16), V((4, PEERS, ROWS, 128), bf16),
            V((4, PEERS, ROWS, 128), bf16), V((PEERS, ROWS, 128), bf16), V((4, ROWS, 128), bf16),
            V((NX, 64, WIDTH), bf16), V((SEQS, GROUPS, GW, STATE), bf16),
            V((NZ, ROWS, WIDTH), bf16), V((NX, 32, 128), bf16),
            V((SEQS, PROPS, WIDTH), bf16), V((SEQS, PROPS, BC), bf16),
            V((SEQS, PROPS, HEADS), f32), V((7, SEQS, WIDTH), bf16), V((SEQS, 7, 2, BC), bf16),
            pltpu.SMEM((SEQS,), i32), DMA((21,)), DMA((15,)), DMA((15,)), DMA((7,)),
            pltpu.SemaphoreType.REGULAR((3, 2)),
        ],
        compiler_params=pltpu.CompilerParams(
            collective_id=0, has_side_effects=True, vmem_limit_bytes=60 * 1024 * 1024
        ),
    )(
        tokens, input_norm_gain, head_input_weight, output_gate_weight, state_maps_weight,
        step_size_weight.T, step_size_bias, head_decay_speed, proposal_decay_total,
        head_input_kernel, state_maps_kernel, head_direct_gain, grouped_norm_gain,
        output_weight.T, prior_state_value, previous_head_input, previous_input_maps,
        previous_log_decays, jnp.transpose(prior_heads_window, (1, 0, 2)), prior_maps_window,
        accepted,
    )
    finals = (jax.ShapeDtypeStruct((64, PROPS, 64), bf16), *outs[1:])
    mixed, state, chi, cim, cld, chw, cmw = pl.pallas_call(
        finish,
        out_shape=finals,
        in_specs=[anywhere] * 7,
        out_specs=[anywhere] * 7,
        scratch_shapes=[
            V((NX * NT, 32, 128), bf16), V((64, PROPS, 64), bf16),
            *(V(o.shape, o.dtype) for o in outs[1:]), DMA((20,)),
        ],
    )(*results)
    return mixed, state, chi, cim, cld, jnp.transpose(chw, (1, 0, 2)), cmw


def solution(mesh):
    seq = ("dp", "kv")
    return jax.shard_map(
        local,
        mesh=mesh,
        in_specs=(
            P("dp", None, "kv"), P(), P("kv", "tp"), P("kv", "tp"), P("kv", None, "tp"), P(), P(),
            P(), P(seq, None, "tp"), P(), P(), P(), P(), P("tp", "kv"), P(seq, "tp", None, None),
            P(seq, None, "tp"), P(seq, None, "tp"), P(seq, None, "tp"), P(seq, None, "tp"),
            P(seq, None, None, "tp"), P(seq),
        ),
        out_specs=(
            P("dp", None, "kv"), P(seq, "tp", None, None), P(seq, None, "tp"), P(seq, None, "tp"),
            P(seq, None, "tp"), P(seq, None, "tp"), P(seq, None, None, "tp"),
        ),
        check_vma=False,
    )
```

time: 47 us -> 44 us (0.936)
  Pallas kernels: 46.2 us -> 43.2 us
    pallas_call x1, Pallas kernels: 43.5 us -> 40.8 us  [local(): pl.pallas_call(kernel, out_shape=outs, in_specs=[anywhere] * 21, out_spec...]
where the time goes in v3:
time: 44 us; the launch traced here: 43.9 us
  Pallas kernels  43.2 us (98%)
  between operations  0.65 us (1%)
    pallas_call x1, Pallas kernels, local(): pl.pallas_call(kernel, out_shape=outs, in_specs=[anywhere] * 21, out_spec...  40.8 us
    pallas_call x1, Pallas kernels, local(): pl.pallas_call(finish, out_shape=finals, in_specs=[anywhere] * 7, out_spe...  2.43 us

profile of v3, /device:TPU:1, one launch (start us, length us, event | category | flops | bytes accessed | tf_op | source)
XLA Modules:
  0.0 43.9 jit_solution(13714776478997931503)
XLA Ops:
  0.6 40.8 %shard_map.252 = (bf16[8,32,128]{2,1,0:T(8,128)(2,1)}, f32[2,24,64,128]{3,2,1,0:T(8,128)}, bf16[2,4,1536]{2,1,0:T(4,128)(2,1)}, bf16[2,4,512]{2,1,0:T(4,128)(2,1...) custom-call(bf16[64,4,64]{2,1,0:T(4,128)(2,1)} %tok_h.1, ...), custom_call_target="tpu_custom_call" | custom-call | tf_op jit(solution)/shard_map/pallas_call | solution.py:536
  41.4 2.4 %shard_map.253 = (bf16[64,4,64]{2,1,0:T(4,128)(2,1)}, f32[2,24,64,128]{3,2,1,0:T(8,128)}, bf16[2,4,1536]{2,1,0:T(4,128)(2,1)}, bf16[2,4,512]{2,1,0:T(4,128)(2,1)...) custom-call(bf16[8,32,128]{2,1,0:T(8,128)(2,1)} %get-tuple-element.21.fr_h, ...), custom_call_target="tpu_custom_call" | custom-call | tf_op jit(solution)/shard_map/pallas_call | solution.py:570

commit v4 on v3

--- a/solution.py
+++ b/solution.py
@@ -69,7 +69,7 @@
     psv_h, phi_h, pim_h, pld_h, phw_h, pmw_h, acc_h,
     fr, state_o, chi_o, cim_o, cld_o, chw_o, cmw_o,
     tok, gain, wxg, smw, ssb, hds, pdt, hik, smk, hdg, gng, wo, psv, phi, pim, pld, phw, pmw,
-    sw, bcs, tt, lhs, wr, send, got, steps_out, steps_in, wor, sb, nrm, fs,
+    sw, bcs, tt, squares_out, squares_in, lhs, wr, send, got, steps_out, steps_in, wor, sb, nrm, last, fs,
     chi, cim, cld, chw, cmw, acc_s, lsem, ssem, rsem, osem, level_sem,
 ):
     y, kv, t = lax.axis_index("dp"), lax.axis_index("kv"), lax.axis_index("tp")
@@ -94,6 +94,7 @@
     )
     for n, (src, dst) in enumerate(plan):
         loads[n] = pltpu.make_async_copy(src, dst, lsem.at[n])
+    for n in (0, 1, 2):
         loads[n].start()
 
     barrier = pltpu.get_barrier_semaphore()
@@ -111,6 +112,10 @@
         pl.semaphore_signal(barrier, inc=1, **at(z, lax.rem(x + d, NX), 1 - t))
     for d in range(1, NY):
         pl.semaphore_signal(barrier, inc=1, **over(d))
+    for d in range(1, NX):
+        pl.semaphore_signal(barrier, inc=1, **at(lax.rem(z + 2 * d, NZ), x, t))
+    for n in range(3, len(plan)):
+        loads[n].start()
 
     for n in (0, 1, 2):
         loads[n].wait()
@@ -124,7 +129,7 @@
     sumsq = jnp.sum(jnp.square(tok32.T), axis=0, keepdims=True)
     high = sumsq.astype(bf16).astype(f32)
     line = iota((16, 256), 0)
-    tt[x, 64:80] = jnp.where(
+    squares_out[...] = jnp.where(
         line == 0, high, jnp.where(line == 1, sumsq - high, 0.0)
     ).astype(bf16)
     for n in range(2):
@@ -145,19 +150,27 @@
     for c in range(4):
         wr[c, x] = columns(c, half, x)[...]
 
-    pl.semaphore_wait(barrier, 11 + NX + NY - 1)
-
-    lanes_t = pl.ds(pl.multiple_of(t * 128, 128), 128)
-    for peers, base in ((up_peers, 8), (down_peers, 4), (row_peers, 0)):
-        for dz, dx in peers:
-            pltpu.make_async_remote_copy(
-                tt.at[x, :, lanes_t],
-                tt.at[base + x, :, lanes_t],
-                ssem.at[4],
-                rsem.at[4],
-                **near(dz, dx)[1],
-            ).start()
-    for c in range(4):
+    pl.semaphore_wait(barrier, 11 + NX + NY - 1 + NX - 1)
+
+    def pass_on(level):
+        for n, dz in enumerate((1, NZ - 1)):
+            pl.semaphore_signal(level_sem.at[level, n], inc=1, **near(dz, 0)[1])
+
+    def hear(level):
+        for n in range(2):
+            pl.semaphore_wait(level_sem.at[level, n], 1)
+
+    pass_on(0)
+
+    @pl.when(t == 1)
+    def _():
+        for peers, base in ((up_peers, 8), (down_peers, 4), (row_peers, 0)):
+            for dz, dx in peers:
+                pltpu.make_async_remote_copy(
+                    tt.at[x], tt.at[base + x], ssem.at[4], rsem.at[4], **near(dz, dx)[1]
+                ).start()
+
+    def send_weights(c):
         for peers, h, base in (
             (down_peers if c < 2 else up_peers, 1 - half, 4),
             (row_peers, half, 0),
@@ -168,37 +181,18 @@
                     columns(c, h, xx), wr.at[c, base + x], ssem.at[c], rsem.at[c], **to
                 ).start()
 
-    def pass_on(level):
-        for n, dz in enumerate((1, NZ - 1)):
-            pl.semaphore_signal(level_sem.at[level, n], inc=1, **near(dz, 0)[1])
-
-    def hear(level):
-        for n in range(2):
-            pl.semaphore_wait(level_sem.at[level, n], 1)
-
-    pass_on(0)
+    steps_mine = (half == 0) & (x == pair)
+
+    @pl.when(jnp.logical_not(steps_mine))
+    def _():
+        pltpu.make_async_remote_copy(
+            squares_out, squares_in.at[half * NX + x], ssem.at[15], rsem.at[15],
+            **at(2 * pair, pair, t),
+        ).start()
 
     def arrived(buffer, count, sem):
         block = buffer.at[pl.ds(0, count)]
         pltpu.make_async_copy(block, block, sem).wait()
-
-    from_me = (x * 2 + half) * 4 + pair
-
-    def spread(src, dst, index, n):
-        def one(d, _):
-            other = lax.rem(kv + d, PEERS)
-            pltpu.make_async_remote_copy(
-                src.at[other],
-                dst.at[index],
-                ssem.at[n],
-                rsem.at[n],
-                device_id=(y, other, t),
-                device_id_type=MESH,
-            ).start()
-            return 0
-
-        lax.fori_loop(1, PEERS, one, 0)
-        dst[index] = src[kv]
 
     loads[20].wait()
     acc = (acc_s[0], acc_s[1])
@@ -220,10 +214,10 @@
     keys = pim[...].astype(f32).reshape(ROWS, BC)
     loads[19].wait()
     for b in range(SEQS):
-        mine = (row >> 2) == b
-        logs = mm(jnp.where(mine, kept, 0.0), jnp.ones((ROWS, STATE), f32), 0, 0, precision=HI)
+        of_b = (row >> 2) == b
+        logs = mm(jnp.where(of_b, kept, 0.0), jnp.ones((ROWS, STATE), f32), 0, 0, precision=HI)
         factor = jnp.exp(logs)
-        keys_b = jnp.where(mine, keys, 0.0)
+        keys_b = jnp.where(of_b, keys, 0.0)
         keys_b = jnp.concatenate([keys_b, keys_b], axis=0).astype(bf16)
         for g in range(GROUPS):
             upd = mm(
@@ -243,31 +237,82 @@
 
     put(0, psv, state_o)
 
+    @pl.when(t == 1)
+    def _():
+        arrived(tt, 11, ssem.at[4])
+
+    for c in range(4):
+        send_weights(c)
+    loads[13].wait()
+    wor[0] = wo[...]
+    mine = pl.ds(pl.multiple_of(y * 16, 16), 16)
+    for d in (2, 1, 3):
+        pltpu.make_async_remote_copy(
+            wo.at[mine], wor.at[NX - d, mine], ssem.at[10], rsem.at[10],
+            **at(lax.rem(z + 2 * d, NZ), x, t),
+        ).start()
+    quarters = wor.at[:, pl.ds(0, 16)]
+    three_quarters = wor.at[:, pl.ds(0, 48)]
+
+    from_me = (x * 2 + half) * 4 + pair
+
+    def spread(src, dst, index, n):
+        def one(d, _):
+            other = lax.rem(kv + d, PEERS)
+            pltpu.make_async_remote_copy(
+                src.at[other],
+                dst.at[index],
+                ssem.at[n],
+                rsem.at[n],
+                device_id=(y, other, t),
+                device_id_type=MESH,
+            ).start()
+            return 0
+
+        lax.fori_loop(1, PEERS, one, 0)
+        dst[index] = src[kv]
+
     for level in range(3):
         hear(level)
         if level < 2:
             pass_on(level + 1)
 
-    loads[13].wait()
-    wor[x] = wo[...]
-    mine = pl.ds(pl.multiple_of(y * 16, 16), 16)
-    quarters = wor.at[:, pl.ds(0, 16)]
-    three_quarters = wor.at[:, pl.ds(0, 48)]
-
-    steps_mine = (half == 0) & (x == pair)
-    halves = tt.at[:, :, pl.ds(0, 128)]
-    arrived(halves, 11, rsem.at[4])
-    blocks = [tt.at[pl.ds(4, 8), :, lanes_t]]
-    blocks += [tt.at[lax.rem(x + d, NX), :, lanes_t] for d in range(1, NX)]
-    for block in blocks:
-        pltpu.make_async_remote_copy(
-            block, block, ssem.at[14], rsem.at[14], **at(z, x, 1 - t)
-        ).start()
-    arrived(halves, 11, rsem.at[14])
-    lhs[...] = tt[:, 0:64].reshape(768, 256).T
+
+    @pl.when(t == 1)
+    def _():
+        arrived(tt, 11, rsem.at[4])
+        blocks = [tt.at[pl.ds(4, 8)]]
+        blocks += [tt.at[lax.rem(x + d, NX)] for d in range(1, NX)]
+        for block in blocks:
+            pltpu.make_async_remote_copy(
+                block, block, ssem.at[14], rsem.at[14], **at(z, x, 1 - t)
+            ).start()
+
+    @pl.when(t == 0)
+    def _():
+        arrived(tt, 11, rsem.at[14])
+
+    lhs[...] = tt[...].reshape(768, 256).T
+    loads[5].wait()
+
+    @pl.when(steps_mine)
+    def _():
+        steps = mm(lhs[:, 0:512], sw[...], 1, 1)
+        arrived(squares_in, 7, rsem.at[15])
+        squares_in[half * NX + x] = squares_out[...]
+        squares = jnp.sum(squares_in[...].astype(f32), axis=0)
+        pick = jnp.where(
+            (iota((16, 128), 1) == 64) & (iota((16, 128), 0) < 2), 1.0, 0.0
+        )
+        squares = mm(squares, pick, 0, 0, precision=HI)
+        total = squares[:, 64:65]
+        high = total.astype(bf16).astype(f32)
+        lane = iota((256, 128), 1)
+        steps = jnp.where(lane == 64, high, jnp.where(lane == 65, total - high, steps))
+        steps_out[...] = steps.reshape(PEERS, ROWS, 128).astype(bf16)
+        spread(steps_out, steps_in, pair, 9)
+
     for c in range(4):
-        if c == 0:
-            loads[5].wait()
         arrived(wr.at[c], 7, rsem.at[c])
         if c < 2:
             part = mm(lhs[:, 0:512], wr[c].reshape(512, 128))
@@ -276,33 +321,10 @@
             part = part + mm(lhs[:, 512:768], wr[c, 4:8].reshape(256, 128))
         send[c] = part.reshape(PEERS, ROWS, 128).astype(bf16)
         spread(send.at[c], got.at[c], from_me, 5 + c)
-        if c == 1:
-            for d in (2, 1, 3):
-                pltpu.make_async_remote_copy(
-                    wo.at[mine], wor.at[x, mine], ssem.at[10], rsem.at[10],
-                    **at(z, lax.rem(x + d, NX), t),
-                ).start()
-        if c == 0:
-
-            @pl.when(steps_mine)
-            def _():
-                steps = mm(lhs[:, 0:512], sw[...], 1, 1)
-                squares = jnp.sum(tt[0:8, 64:80].astype(f32), axis=0)
-                pick = jnp.where(
-                    (iota((16, 128), 1) == 64) & (iota((16, 128), 0) < 2), 1.0, 0.0
-                )
-                squares = mm(squares, pick, 0, 0, precision=HI)
-                total = squares[:, 64:65]
-                high = total.astype(bf16).astype(f32)
-                lane = iota((256, 128), 1)
-                steps = jnp.where(lane == 64, high, jnp.where(lane == 65, total - high, steps))
-                steps_out[...] = steps.reshape(PEERS, ROWS, 128).astype(bf16)
-                spread(steps_out, steps_in, pair, 9)
-
     arrived(quarters, 3, rsem.at[10])
     for d in (2, 1, 3):
         for e in (2, 1, 3):
-            block = wor.at[lax.rem(x + d, NX), mine]
+            block = wor.at[d, mine]
             pltpu.make_async_remote_copy(
                 block, block, ssem.at[13], rsem.at[13], **over(e)
             ).start()
@@ -397,7 +419,17 @@
             [v[:, g * 128 : g * 128 + 128] for g in range(GROUPS) for v in thirds], axis=1
         )
 
-    windows, inputs, gated = [], [], []
+    slot = half * NX + x
+
+    def to_pair(block, n):
+        for dx, dp in ((2, 1), (2, 0), (1, 1), (3, 1), (1, 0), (3, 0), (0, 1)):
+            pltpu.make_async_remote_copy(
+                block, block, ssem.at[n], rsem.at[n],
+                **at(2 * pair + lax.rem(half + dp, 2), lax.rem(x + dx, NX), t),
+            ).start()
+
+    windows, inputs = [], []
+    energy = [0.0] * GROUPS
     for c in range(1, 4):
         wide_c, taps_c, old_c = third(wide, c), third(taps_x, c), third(old_x, c)
         cum_w, step_w, direct_w = wide_c[0:8], wide_c[8:16], wide_c[16:24]
@@ -422,44 +454,74 @@
         for d in range(1, PROPS):
             term = decay_w[d] * pltpu.roll(weighted, d, 0)
             heads = heads + jnp.where((row & 3) >= d, term, 0.0)
-        gated.append(heads * (gate * lax.logistic(gate)))
-
-    gated = whole(gated)
-    normed = []
-    for g in range(GROUPS):
-        part_g = gated[:, g * GW : g * GW + GW]
-        mean = jnp.sum(part_g * part_g, axis=1, keepdims=True) / GW
-        normed.append(part_g * lax.rsqrt(mean + eps))
-    nrm[z] = (jnp.concatenate(normed, axis=1) * out_gain).astype(bf16)
-    for d in (4, 3, 5, 2, 6, 1, 7):
-        pltpu.make_async_remote_copy(
-            nrm.at[z], nrm.at[z], ssem.at[11], rsem.at[11], **at(lax.rem(z + d, NZ), x, t)
-        ).start()
+        gated = heads * (gate * lax.logistic(gate))
+        for g in range(GROUPS):
+            part_g = gated[:, g * 128 : g * 128 + 128]
+            energy[g] = energy[g] + jnp.sum(part_g * part_g, axis=1, keepdims=True)
+        gated = gated * third(out_gain, c)
+        if c < 3:
+            nrm[c - 1, slot] = gated.astype(bf16)
+            to_pair(nrm.at[c - 1, slot], 15 + c)
+            continue
+        factors = jnp.zeros((ROWS, 128), f32)
+        for g in range(GROUPS):
+            factor = lax.rsqrt(energy[g] / GW + eps)
+            high = factor.astype(bf16).astype(f32)
+            factors = jnp.where(lane8 == g, high, factors)
+            factors = jnp.where(lane8 == GROUPS + g, factor - high, factors)
+        last[slot] = jnp.concatenate([gated, factors], axis=1).astype(bf16)
+        to_pair(last.at[slot], 18)
     chw[...] = whole(windows).reshape(7, SEQS, WIDTH).astype(bf16)
     put(4, chw, chw_o)
     chi[...] = whole(inputs).reshape(SEQS, PROPS, WIDTH).astype(bf16)
     put(5, chi, chi_o)
 
     arrived(three_quarters, 3, rsem.at[13])
-    arrived(nrm, 7, rsem.at[11])
-    rows64 = nrm[...].astype(f32).reshape(64, WIDTH).astype(bf16)
-    for d in (2, 1, 3, 0):
-        xp = lax.rem(x + d, NX)
-        part = mm(rows64, wor[xp], 1, 1)
-        fs[d] = jnp.concatenate([part[:32], part[32:]], axis=1).astype(bf16)
+    columns_of = wor[...].reshape(256, WIDTH)
+    products = [jnp.zeros((64, 256), f32)] * GROUPS
+    for c in range(1, 4):
+        if c < 3:
+            arrived(nrm.at[c - 1], 7, rsem.at[15 + c])
+            rows64 = nrm[c - 1].astype(f32).reshape(64, 512).astype(bf16)
+        else:
+            arrived(last, 7, rsem.at[18])
+            rows64 = last[:, :, 0:512].astype(f32).reshape(64, 512).astype(bf16)
+        for g in range(GROUPS):
+            start = g * GW + (c - 1) * 128
+            products[g] = products[g] + mm(
+                rows64[:, g * 128 : g * 128 + 128], columns_of[:, start : start + 128], 1, 1
+            )
+    factors = last[:, :, 512:640].astype(f32).reshape(64, 128)
+    factors = factors + pltpu.roll(factors, 128 - GROUPS, 1)
+    partial = factors[:, 0:1] * products[0]
+    for g in range(1, GROUPS):
+        partial = partial + factors[:, g : g + 1] * products[g]
+    first_lanes = iota((32, 128), 1) < 64
+    for d in (2, 3, 1, 0):
+        both = partial[:, 128 * (d // 2) : 128 * (d // 2) + 128]
+        turned = pltpu.roll(both, 64, 1)
+        low, high = (both, turned) if d % 2 == 0 else (turned, both)
+        fs[d] = jnp.where(first_lanes, low[:32], high[32:]).astype(bf16)
+        zz, there = lax.rem(z + 2 * d, NZ), fr.at[pair * NT + t]
         if d == 0:
-            put(6, fs.at[0], fr.at[x * NT + t])
+            put(6, fs.at[0], there)
         else:
             pltpu.make_async_remote_copy(
-                fs.at[d], fr.at[x * NT + t], ssem.at[12], rsem.at[12], **at(z, xp, t)
+                fs.at[d], there, ssem.at[12], rsem.at[12], **at(zz, x, t)
             ).start()
         pltpu.make_async_remote_copy(
-            fs.at[d], fr.at[x * NT + t], ssem.at[12], rsem.at[12], **at(z, xp, 1 - t)
+            fs.at[d], there, ssem.at[12], rsem.at[12], **at(zz, x, 1 - t)
         ).start()
     arrived(fr, 7, rsem.at[12])
 
-    arrived(halves, 11, ssem.at[4])
-    arrived(halves, 11, ssem.at[14])
+    @pl.when(t == 1)
+    def _():
+        arrived(tt, 11, ssem.at[14])
+
+    @pl.when(jnp.logical_not(steps_mine))
+    def _():
+        pltpu.make_async_copy(squares_out, squares_out, ssem.at[15]).wait()
+
     for c in range(4):
         arrived(wr.at[c], 7, ssem.at[c])
         arrived(send.at[c], PEERS - 1, ssem.at[5 + c])
@@ -470,7 +532,9 @@
 
     arrived(quarters, 3, ssem.at[10])
     arrived(three_quarters, 3, ssem.at[13])
-    arrived(nrm, 7, ssem.at[11])
+    for c in range(2):
+        arrived(nrm.at[c], 7, ssem.at[16 + c])
+    arrived(last, 7, ssem.at[18])
     arrived(fr, 7, ssem.at[12])
     for copy in outs:
         copy.wait()
@@ -485,7 +549,7 @@
     def pieces(ref, n):
         if n > 0:
             return [ref]
-        return [ref.at[b, pl.ds(h, 12)] for b in range(SEQS) for h in (0, 12)]
+        return [ref.at[b, pl.ds(h, 6)] for b in range(SEQS) for h in range(0, HEADS, 6)]
 
     trio = [
         piece
@@ -495,17 +559,15 @@
     head = pltpu.make_async_copy(fr_h, fr, sems.at[0])
     head.start()
     first = [pltpu.make_async_copy(a, b, sems.at[1 + n]) for n, (a, b, _) in enumerate(trio)]
-    second = [pltpu.make_async_copy(b, c, sems.at[10 + n]) for n, (_, b, c) in enumerate(trio)]
+    second = [pltpu.make_async_copy(b, c, sems.at[14 + n]) for n, (_, b, c) in enumerate(trio)]
     for copy in first:
         copy.start()
     head.wait()
-    done = fr[...].astype(f32).reshape(NX, NT, 32, 128)
-    done = (done[:, 0] + done[:, 1]).reshape(NX, 4, ROWS, 128)
-    done = jnp.stack(
-        [done[:, n % 4, :, :64] if n < 4 else done[:, n % 4, :, 64:] for n in range(NZ)], axis=0
-    )
+    done = fr[...].astype(f32).reshape(4, NT, 32, 128)
+    done = done[:, 0] + done[:, 1]
+    done = jnp.stack([done[:, :, :64], done[:, :, 64:]], axis=1)
     mixed[...] = done.reshape(64, PROPS, 64).astype(bf16)
-    last = pltpu.make_async_copy(mixed, mixed_o, sems.at[19])
+    last = pltpu.make_async_copy(mixed, mixed_o, sems.at[27])
     last.start()
     for a, b in zip(first, second):
         a.wait()
@@ -545,14 +607,14 @@
             V((64, WIDTH), bf16), V((SEQS, HEADS, HEAD_DIM, STATE), f32),
             V((SEQS, PROPS, WIDTH), bf16), V((SEQS, PROPS, BC), bf16),
             V((SEQS, PROPS, HEADS), f32), V((7, SEQS, WIDTH), bf16), V((SEQS, 7, 2, BC), bf16),
-            V((128, 512), bf16), V((8, 64, 128), bf16), V((12, 80, 256), bf16),
+            V((128, 512), bf16), V((8, 64, 128), bf16), V((12, 64, 256), bf16), V((16, 256), bf16), V((8, 16, 256), bf16),
             V((256, 768), bf16), V((4, 8, 64, 128), bf16), V((4, PEERS, ROWS, 128), bf16),
             V((4, PEERS, ROWS, 128), bf16), V((PEERS, ROWS, 128), bf16), V((4, ROWS, 128), bf16),
             V((NX, 64, WIDTH), bf16), V((SEQS, GROUPS, GW, STATE), bf16),
-            V((NZ, ROWS, WIDTH), bf16), V((NX, 32, 128), bf16),
+            V((2, 8, ROWS, 512), bf16), V((8, ROWS, 640), bf16), V((NX, 32, 128), bf16),
             V((SEQS, PROPS, WIDTH), bf16), V((SEQS, PROPS, BC), bf16),
             V((SEQS, PROPS, HEADS), f32), V((7, SEQS, WIDTH), bf16), V((SEQS, 7, 2, BC), bf16),
-            pltpu.SMEM((SEQS,), i32), DMA((21,)), DMA((15,)), DMA((15,)), DMA((7,)),
+            pltpu.SMEM((SEQS,), i32), DMA((21,)), DMA((19,)), DMA((19,)), DMA((7,)),
             pltpu.SemaphoreType.REGULAR((3, 2)),
         ],
         compiler_params=pltpu.CompilerParams(
@@ -574,7 +636,7 @@
         out_specs=[anywhere] * 7,
         scratch_shapes=[
             V((NX * NT, 32, 128), bf16), V((64, PROPS, 64), bf16),
-            *(V(o.shape, o.dtype) for o in outs[1:]), DMA((20,)),
+            *(V(o.shape, o.dtype) for o in outs[1:]), DMA((28,)),
         ],
     )(*results)
     return mixed, state, chi, cim, cld, jnp.transpose(chw, (1, 0, 2)), cmw

time: 44 us -> 42.2 us (0.959)
  Pallas kernels: 43.2 us -> 41.3 us
    pallas_call x1, Pallas kernels: 40.8 us -> 38.8 us  [local(): pl.pallas_call(kernel, out_shape=outs, in_specs=[anywhere] * 21, out_spec...]
where the time goes in v4:
time: 42.2 us; the launch traced here: 41.9 us
  Pallas kernels  41.3 us (98%)
  between operations  0.65 us (2%)
    pallas_call x1, Pallas kernels, local(): pl.pallas_call(kernel, out_shape=outs, in_specs=[anywhere] * 21, out_spec...  38.8 us
    pallas_call x1, Pallas kernels, local(): pl.pallas_call(finish, out_shape=finals, in_specs=[anywhere] * 7, out_spe...  2.49 us

profile of v4, /device:TPU:1, one launch (start us, length us, event | category | flops | bytes accessed | tf_op | source)
XLA Modules:
  0.0 41.9 jit_solution(5933910100021775858)
XLA Ops:
  0.6 38.8 %shard_map.252 = (bf16[8,32,128]{2,1,0:T(8,128)(2,1)}, f32[2,24,64,128]{3,2,1,0:T(8,128)}, bf16[2,4,1536]{2,1,0:T(4,128)(2,1)}, bf16[2,4,512]{2,1,0:T(4,128)(2,1...) custom-call(bf16[64,4,64]{2,1,0:T(4,128)(2,1)} %tok_h.1, ...), custom_call_target="tpu_custom_call" | custom-call | tf_op jit(solution)/shard_map/pallas_call | solution.py:598
  39.4 2.5 %shard_map.253 = (bf16[64,4,64]{2,1,0:T(4,128)(2,1)}, f32[2,24,64,128]{3,2,1,0:T(8,128)}, bf16[2,4,1536]{2,1,0:T(4,128)(2,1)}, bf16[2,4,512]{2,1,0:T(4,128)(2,1)...) custom-call(bf16[8,32,128]{2,1,0:T(8,128)(2,1)} %get-tuple-element.21.fr_h, ...), custom_call_target="tpu_custom_call" | custom-call | tf_op jit(solution)/shard_map/pallas_call | solution.py:632

commit v5 on v4

--- a/solution.py
+++ b/solution.py
@@ -67,10 +67,10 @@
 def kernel(
     tok_h, gain_h, wx_h, wg_h, smw_h, sw_h, ssb_h, hds_h, pdt_h, hik_h, smk_h, hdg_h, gng_h, wo_h,
     psv_h, phi_h, pim_h, pld_h, phw_h, pmw_h, acc_h,
-    fr, state_o, chi_o, cim_o, cld_o, chw_o, cmw_o,
+    fr, state, chi, cim, cld, chw, cmw,
     tok, gain, wxg, smw, ssb, hds, pdt, hik, smk, hdg, gng, wo, psv, phi, pim, pld, phw, pmw,
     sw, bcs, tt, squares_out, squares_in, lhs, wr, send, got, steps_out, steps_in, wor, sb, nrm, last, fs,
-    chi, cim, cld, chw, cmw, acc_s, lsem, ssem, rsem, osem, level_sem,
+    acc_s, lsem, ssem, rsem, level_sem,
 ):
     y, kv, t = lax.axis_index("dp"), lax.axis_index("kv"), lax.axis_index("tp")
     z, x = kv // NX, kv % NX
@@ -81,6 +81,12 @@
 
     def over(d):
         return dict(device_id=(lax.rem(y + d, NY), kv, t), device_id_type=MESH)
+
+    def served(e):
+        return lax.rem(z + (2 * half - 1) * e + NZ, NZ)
+
+    def server(e):
+        return lax.rem(z + (1 - 2 * ((half + e) % 2)) * e + NZ, NZ)
 
     loads = {}
     plan = (
@@ -112,8 +118,8 @@
         pl.semaphore_signal(barrier, inc=1, **at(z, lax.rem(x + d, NX), 1 - t))
     for d in range(1, NY):
         pl.semaphore_signal(barrier, inc=1, **over(d))
-    for d in range(1, NX):
-        pl.semaphore_signal(barrier, inc=1, **at(lax.rem(z + 2 * d, NZ), x, t))
+    for e in (2, 3):
+        pl.semaphore_signal(barrier, inc=1, **at(served(e), x, t))
     for n in range(3, len(plan)):
         loads[n].start()
 
@@ -150,7 +156,7 @@
     for c in range(4):
         wr[c, x] = columns(c, half, x)[...]
 
-    pl.semaphore_wait(barrier, 11 + NX + NY - 1 + NX - 1)
+    pl.semaphore_wait(barrier, 11 + NX + NY - 1 + 2)
 
     def pass_on(level):
         for n, dz in enumerate((1, NZ - 1)):
@@ -180,6 +186,20 @@
                 pltpu.make_async_remote_copy(
                     columns(c, h, xx), wr.at[c, base + x], ssem.at[c], rsem.at[c], **to
                 ).start()
+
+    loads[13].wait()
+    wor[0] = wo[...]
+    mine = pl.ds(pl.multiple_of(y * 16, 16), 16)
+
+    def send_output_weights():
+        for e in (3, 2, 1):
+            pltpu.make_async_remote_copy(
+                wo.at[mine], wor.at[e, mine], ssem.at[10], rsem.at[10], **at(server(e), x, t)
+            ).start()
+
+    @pl.when(t == 0)
+    def _():
+        send_output_weights()
 
     steps_mine = (half == 0) & (x == pair)
 
@@ -227,15 +247,8 @@
                 psv[b, g * PER : g * PER + PER] * factor[g * PER : g * PER + PER][:, None, :]
                 + upd.reshape(PER, HEAD_DIM, STATE)
             )
-            psv[b, g * PER : g * PER + PER] = new
+            state[b, g * PER : g * PER + PER] = new
             sb[b, g] = new.reshape(GW, STATE).astype(bf16)
-    outs = []
-
-    def put(n, src, dst):
-        outs.append(pltpu.make_async_copy(src, dst, osem.at[n]))
-        outs[-1].start()
-
-    put(0, psv, state_o)
 
     @pl.when(t == 1)
     def _():
@@ -243,14 +256,10 @@
 
     for c in range(4):
         send_weights(c)
-    loads[13].wait()
-    wor[0] = wo[...]
-    mine = pl.ds(pl.multiple_of(y * 16, 16), 16)
-    for d in (2, 1, 3):
-        pltpu.make_async_remote_copy(
-            wo.at[mine], wor.at[NX - d, mine], ssem.at[10], rsem.at[10],
-            **at(lax.rem(z + 2 * d, NZ), x, t),
-        ).start()
+    @pl.when(t == 1)
+    def _():
+        send_output_weights()
+
     quarters = wor.at[:, pl.ds(0, 16)]
     three_quarters = wor.at[:, pl.ds(0, 48)]
 
@@ -369,7 +378,6 @@
     raw_c = jnp.concatenate([sum0[g, 1] for g in range(GROUPS)], axis=1) * inv
     win_bc = mm(pick_bc, jnp.concatenate([old_bc, raw_b, raw_c], axis=0).astype(bf16))
     cmw[...] = win_bc[64:92].reshape(SEQS, 7, 2, BC).astype(bf16)
-    put(1, cmw, cmw_o)
     b_conv = taps_bc[0:1] * win_bc[0:8]
     c_conv = taps_bc[1:2] * win_bc[8:16]
     for k in range(1, 4):
@@ -388,9 +396,7 @@
         precision=HI,
     )
     cim[...] = b_conv.reshape(SEQS, PROPS, BC).astype(bf16)
-    put(2, cim, cim_o)
     cld[...] = decays.reshape(SEQS, PROPS, HEADS)
-    put(3, cld, cld_o)
     from_state, pairs = [], []
     for g in range(GROUPS):
         lanes = slice(g * STATE, g * STATE + STATE)
@@ -472,9 +478,7 @@
         last[slot] = jnp.concatenate([gated, factors], axis=1).astype(bf16)
         to_pair(last.at[slot], 18)
     chw[...] = whole(windows).reshape(7, SEQS, WIDTH).astype(bf16)
-    put(4, chw, chw_o)
     chi[...] = whole(inputs).reshape(SEQS, PROPS, WIDTH).astype(bf16)
-    put(5, chi, chi_o)
 
     arrived(three_quarters, 3, rsem.at[13])
     columns_of = wor[...].reshape(256, WIDTH)
@@ -497,14 +501,14 @@
     for g in range(1, GROUPS):
         partial = partial + factors[:, g : g + 1] * products[g]
     first_lanes = iota((32, 128), 1) < 64
-    for d in (2, 3, 1, 0):
+    for d in (3, 2, 1, 0):
         both = partial[:, 128 * (d // 2) : 128 * (d // 2) + 128]
         turned = pltpu.roll(both, 64, 1)
         low, high = (both, turned) if d % 2 == 0 else (turned, both)
         fs[d] = jnp.where(first_lanes, low[:32], high[32:]).astype(bf16)
-        zz, there = lax.rem(z + 2 * d, NZ), fr.at[pair * NT + t]
+        zz, there = served(d), fr.at[pair * NT + t]
         if d == 0:
-            put(6, fs.at[0], there)
+            fr[pair * NT + t] = fs[0]
         else:
             pltpu.make_async_remote_copy(
                 fs.at[d], there, ssem.at[12], rsem.at[12], **at(zz, x, t)
@@ -536,45 +540,23 @@
         arrived(nrm.at[c], 7, ssem.at[16 + c])
     arrived(last, 7, ssem.at[18])
     arrived(fr, 7, ssem.at[12])
-    for copy in outs:
-        copy.wait()
-
-
-def finish(fr_h, *refs):
-    ins, outs, fr, mixed, mids, sems = (
-        refs[:6], refs[7:13], refs[13], refs[14], refs[15:21], refs[21],
-    )
-    mixed_o = refs[6]
-
-    def pieces(ref, n):
-        if n > 0:
-            return [ref]
-        return [ref.at[b, pl.ds(h, 6)] for b in range(SEQS) for h in range(0, HEADS, 6)]
-
-    trio = [
-        piece
-        for n in (1, 2, 3, 4, 5, 0)
-        for piece in zip(pieces(ins[n], n), pieces(mids[n], n), pieces(outs[n], n))
+
+
+def finish(fr, *refs):
+    ins, outs, mixed, sems = refs[:6], refs[6:13], refs[13], refs[14]
+    copies = [
+        pltpu.make_async_copy(a, b, sems.at[n]) for n, (a, b) in enumerate(zip(ins, outs[1:]))
     ]
-    head = pltpu.make_async_copy(fr_h, fr, sems.at[0])
-    head.start()
-    first = [pltpu.make_async_copy(a, b, sems.at[1 + n]) for n, (a, b, _) in enumerate(trio)]
-    second = [pltpu.make_async_copy(b, c, sems.at[14 + n]) for n, (_, b, c) in enumerate(trio)]
-    for copy in first:
+    for copy in copies:
         copy.start()
-    head.wait()
     done = fr[...].astype(f32).reshape(4, NT, 32, 128)
     done = done[:, 0] + done[:, 1]
     done = jnp.stack([done[:, :, :64], done[:, :, 64:]], axis=1)
     mixed[...] = done.reshape(64, PROPS, 64).astype(bf16)
-    last = pltpu.make_async_copy(mixed, mixed_o, sems.at[27])
-    last.start()
-    for a, b in zip(first, second):
-        a.wait()
-        b.start()
-    for copy in second:
+    copies.append(pltpu.make_async_copy(mixed, outs[0], sems.at[6]))
+    copies[-1].start()
+    for copy in copies:
         copy.wait()
-    last.wait()
 
 
 def local(
@@ -585,6 +567,7 @@
     prior_maps_window, accepted,
 ):
     anywhere = pl.BlockSpec(memory_space=pl.ANY)
+    vmem = pl.BlockSpec(memory_space=pltpu.VMEM)
     V, DMA = pltpu.VMEM, pltpu.SemaphoreType.DMA
     outs = (
         jax.ShapeDtypeStruct((NX * NT, 32, 128), bf16),
@@ -595,11 +578,14 @@
         jax.ShapeDtypeStruct((7, SEQS, WIDTH), bf16),
         jax.ShapeDtypeStruct((SEQS, 7, 2, BC), bf16),
     )
+    def in_hbm(v):
+        return pltpu.with_memory_space_constraint(v, pltpu.HBM)
+
     results = pl.pallas_call(
         kernel,
         out_shape=outs,
         in_specs=[anywhere] * 21,
-        out_specs=[anywhere] * 7,
+        out_specs=[vmem] * 7,
         scratch_shapes=[
             V((64, PROPS, 64), bf16), V((D,), bf16), V((2, 64, WIDTH), bf16),
             V((64, 2, BC), bf16), V((48,), f32), V((48,), f32), V((SEQS, PROPS, HEADS), f32),
@@ -612,32 +598,28 @@
             V((4, PEERS, ROWS, 128), bf16), V((PEERS, ROWS, 128), bf16), V((4, ROWS, 128), bf16),
             V((NX, 64, WIDTH), bf16), V((SEQS, GROUPS, GW, STATE), bf16),
             V((2, 8, ROWS, 512), bf16), V((8, ROWS, 640), bf16), V((NX, 32, 128), bf16),
-            V((SEQS, PROPS, WIDTH), bf16), V((SEQS, PROPS, BC), bf16),
-            V((SEQS, PROPS, HEADS), f32), V((7, SEQS, WIDTH), bf16), V((SEQS, 7, 2, BC), bf16),
-            pltpu.SMEM((SEQS,), i32), DMA((21,)), DMA((19,)), DMA((19,)), DMA((7,)),
+            pltpu.SMEM((SEQS,), i32), DMA((21,)), DMA((19,)), DMA((19,)),
             pltpu.SemaphoreType.REGULAR((3, 2)),
         ],
         compiler_params=pltpu.CompilerParams(
-            collective_id=0, has_side_effects=True, vmem_limit_bytes=60 * 1024 * 1024
+            collective_id=0, has_side_effects=True, vmem_limit_bytes=40 * 1024 * 1024
         ),
-    )(
+    )(*(in_hbm(v) for v in (
         tokens, input_norm_gain, head_input_weight, output_gate_weight, state_maps_weight,
         step_size_weight.T, step_size_bias, head_decay_speed, proposal_decay_total,
         head_input_kernel, state_maps_kernel, head_direct_gain, grouped_norm_gain,
         output_weight.T, prior_state_value, previous_head_input, previous_input_maps,
         previous_log_decays, jnp.transpose(prior_heads_window, (1, 0, 2)), prior_maps_window,
         accepted,
-    )
+    )))
     finals = (jax.ShapeDtypeStruct((64, PROPS, 64), bf16), *outs[1:])
     mixed, state, chi, cim, cld, chw, cmw = pl.pallas_call(
         finish,
         out_shape=finals,
-        in_specs=[anywhere] * 7,
+        in_specs=[vmem] * 7,
         out_specs=[anywhere] * 7,
-        scratch_shapes=[
-            V((NX * NT, 32, 128), bf16), V((64, PROPS, 64), bf16),
-            *(V(o.shape, o.dtype) for o in outs[1:]), DMA((28,)),
-        ],
+        scratch_shapes=[V((64, PROPS, 64), bf16), DMA((7,))],
+        compiler_params=pltpu.CompilerParams(vmem_limit_bytes=8 * 1024 * 1024),
     )(*results)
     return mixed, state, chi, cim, cld, jnp.transpose(chw, (1, 0, 2)), cmw
 

time: 42.2 us -> 39.5 us (0.936)
  Pallas kernels: 41.3 us -> 38.7 us
    pallas_call x1, Pallas kernels: 38.8 us -> 37.5 us  [local(): pl.pallas_call(kernel, out_shape=outs, in_specs=[anywhere] * 21, out_spec...]
    pallas_call x1, Pallas kernels: 2.49 us -> 1.25 us  [local(): pl.pallas_call(finish, out_shape=finals, in_specs=[vmem] * 7, out_specs=[...]
where the time goes in v5:
time: 39.5 us; the launch traced here: 39.4 us
  Pallas kernels  38.7 us (98%)
  between operations  0.65 us (2%)
    pallas_call x1, Pallas kernels, local(): pl.pallas_call(kernel, out_shape=outs, in_specs=[anywhere] * 21, out_spec...  37.5 us
    pallas_call x1, Pallas kernels, local(): pl.pallas_call(finish, out_shape=finals, in_specs=[vmem] * 7, out_specs=[...  1.25 us

profile of v5, /device:TPU:1, one launch (start us, length us, event | category | flops | bytes accessed | tf_op | source)
XLA Modules:
  0.0 39.4 jit_solution(1474342421574358979)
XLA Ops:
  0.6 37.5 %shard_map.252 = (bf16[8,32,128]{2,1,0:T(8,128)(2,1)S(1)}, f32[2,24,64,128]{3,2,1,0:T(8,128)S(1)}, bf16[2,4,1536]{2,1,0:T(4,128)(2,1)S(1)}, bf16[2,4,512]{2,1,0:...) custom-call(bf16[64,4,64]{2,1,0:T(4,128)(2,1)} %tok_h.1, ...), custom_call_target="tpu_custom_call" | custom-call | tf_op jit(solution)/shard_map/pallas_call | solution.py:584
  38.1 1.3 %shard_map.253 = (bf16[64,4,64]{2,1,0:T(4,128)(2,1)}, f32[2,24,64,128]{3,2,1,0:T(8,128)}, bf16[2,4,1536]{2,1,0:T(4,128)(2,1)}, bf16[2,4,512]{2,1,0:T(4,128)(2,1)...) custom-call(bf16[8,32,128]{2,1,0:T(8,128)(2,1)S(1)} %get-tuple-element.21.fr, ...), custom_call_target="tpu_custom_call" | custom-call | tf_op jit(solution)/shard_map/pallas_call | solution.py:616

commit v6 on v5

--- a/solution.py
+++ b/solution.py
@@ -249,10 +249,6 @@
             )
             state[b, g * PER : g * PER + PER] = new
             sb[b, g] = new.reshape(GW, STATE).astype(bf16)
-
-    @pl.when(t == 1)
-    def _():
-        arrived(tt, 11, ssem.at[4])
 
     for c in range(4):
         send_weights(c)
@@ -520,6 +516,10 @@
 
     @pl.when(t == 1)
     def _():
+        arrived(tt, 11, ssem.at[4])
+
+    @pl.when(t == 1)
+    def _():
         arrived(tt, 11, ssem.at[14])
 
     @pl.when(jnp.logical_not(steps_mine))

time: 39.5 us -> 39.1 us (0.990)
  Pallas kernels: 38.7 us -> 38.3 us
    pallas_call x1, Pallas kernels: 37.5 us -> 37.1 us  [local(): pl.pallas_call(kernel, out_shape=outs, in_specs=[anywhere] * 21, out_spec...]
where the time goes in v6:
time: 39.1 us; the launch traced here: 39 us
  Pallas kernels  38.3 us (98%)
  between operations  0.65 us (2%)
    pallas_call x1, Pallas kernels, local(): pl.pallas_call(kernel, out_shape=outs, in_specs=[anywhere] * 21, out_spec...  37.1 us
    pallas_call x1, Pallas kernels, local(): pl.pallas_call(finish, out_shape=finals, in_specs=[vmem] * 7, out_specs=[...  1.25 us

profile of v6, /device:TPU:1, one launch (start us, length us, event | category | flops | bytes accessed | tf_op | source)
XLA Modules:
  0.0 39.0 jit_solution(11527494884710587061)
XLA Ops:
  0.6 37.1 %shard_map.252 = (bf16[8,32,128]{2,1,0:T(8,128)(2,1)S(1)}, f32[2,24,64,128]{3,2,1,0:T(8,128)S(1)}, bf16[2,4,1536]{2,1,0:T(4,128)(2,1)S(1)}, bf16[2,4,512]{2,1,0:...) custom-call(bf16[64,4,64]{2,1,0:T(4,128)(2,1)} %tok_h.1, ...), custom_call_target="tpu_custom_call" | custom-call | tf_op jit(solution)/shard_map/pallas_call | solution.py:584
  37.7 1.3 %shard_map.253 = (bf16[64,4,64]{2,1,0:T(4,128)(2,1)}, f32[2,24,64,128]{3,2,1,0:T(8,128)}, bf16[2,4,1536]{2,1,0:T(4,128)(2,1)}, bf16[2,4,512]{2,1,0:T(4,128)(2,1)...) custom-call(bf16[8,32,128]{2,1,0:T(8,128)(2,1)S(1)} %get-tuple-element.21.fr, ...), custom_call_target="tpu_custom_call" | custom-call | tf_op jit(solution)/shard_map/pallas_call | solution.py:616

commit v7 on v6

--- a/solution.py
+++ b/solution.py
@@ -170,11 +170,11 @@
 
     @pl.when(t == 1)
     def _():
-        for peers, base in ((up_peers, 8), (down_peers, 4), (row_peers, 0)):
-            for dz, dx in peers:
-                pltpu.make_async_remote_copy(
-                    tt.at[x], tt.at[base + x], ssem.at[4], rsem.at[4], **near(dz, dx)[1]
-                ).start()
+        turns = [p for two in zip(up_peers, down_peers) for p in zip(two, (8, 4))]
+        for (dz, dx), base in turns + [(p, 0) for p in row_peers]:
+            pltpu.make_async_remote_copy(
+                tt.at[x], tt.at[base + x], ssem.at[4], rsem.at[4], **near(dz, dx)[1]
+            ).start()
 
     def send_weights(c):
         for peers, h, base in (

time: 39.1 us -> 38.9 us (level)
  no operation moved by 1% of the time
where the time goes in v7:
time: 38.9 us; the launch traced here: 38.8 us
  Pallas kernels  38.2 us (98%)
  between operations  0.65 us (2%)
    pallas_call x1, Pallas kernels, local(): pl.pallas_call(kernel, out_shape=outs, in_specs=[anywhere] * 21, out_spec...  36.9 us
    pallas_call x1, Pallas kernels, local(): pl.pallas_call(finish, out_shape=finals, in_specs=[vmem] * 7, out_specs=[...  1.25 us

profile of v7, /device:TPU:1, one launch (start us, length us, event | category | flops | bytes accessed | tf_op | source)
XLA Modules:
  0.0 38.8 jit_solution(2240852406476713786)
XLA Ops:
  0.6 36.9 %shard_map.252 = (bf16[8,32,128]{2,1,0:T(8,128)(2,1)S(1)}, f32[2,24,64,128]{3,2,1,0:T(8,128)S(1)}, bf16[2,4,1536]{2,1,0:T(4,128)(2,1)S(1)}, bf16[2,4,512]{2,1,0:...) custom-call(bf16[64,4,64]{2,1,0:T(4,128)(2,1)} %tok_h.1, ...), custom_call_target="tpu_custom_call" | custom-call | tf_op jit(solution)/shard_map/pallas_call | solution.py:584
  37.6 1.3 %shard_map.253 = (bf16[64,4,64]{2,1,0:T(4,128)(2,1)}, f32[2,24,64,128]{3,2,1,0:T(8,128)}, bf16[2,4,1536]{2,1,0:T(4,128)(2,1)}, bf16[2,4,512]{2,1,0:T(4,128)(2,1)...) custom-call(bf16[8,32,128]{2,1,0:T(8,128)(2,1)S(1)} %get-tuple-element.21.fr, ...), custom_call_target="tpu_custom_call" | custom-call | tf_op jit(solution)/shard_map/pallas_call | solution.py:616

commit v8 on v7

--- a/solution.py
+++ b/solution.py
@@ -173,7 +173,11 @@
         turns = [p for two in zip(up_peers, down_peers) for p in zip(two, (8, 4))]
         for (dz, dx), base in turns + [(p, 0) for p in row_peers]:
             pltpu.make_async_remote_copy(
-                tt.at[x], tt.at[base + x], ssem.at[4], rsem.at[4], **near(dz, dx)[1]
+                tt.at[x],
+                tt.at[base + x],
+                ssem.at[4],
+                rsem.at[{0: 11, 4: 4, 8: 19}[base]],
+                **near(dz, dx)[1],
             ).start()
 
     def send_weights(c):
@@ -285,13 +289,17 @@
 
     @pl.when(t == 1)
     def _():
-        arrived(tt, 11, rsem.at[4])
-        blocks = [tt.at[pl.ds(4, 8)]]
-        blocks += [tt.at[lax.rem(x + d, NX)] for d in range(1, NX)]
-        for block in blocks:
-            pltpu.make_async_remote_copy(
-                block, block, ssem.at[14], rsem.at[14], **at(z, x, 1 - t)
-            ).start()
+        row_blocks = [tt.at[lax.rem(x + d, NX)] for d in range(1, NX)]
+        for count, n, blocks in (
+            (3, 11, row_blocks),
+            (4, 4, [tt.at[pl.ds(4, 4)]]),
+            (4, 19, [tt.at[pl.ds(8, 4)]]),
+        ):
+            arrived(tt, count, rsem.at[n])
+            for block in blocks:
+                pltpu.make_async_remote_copy(
+                    block, block, ssem.at[14], rsem.at[14], **at(z, x, 1 - t)
+                ).start()
 
     @pl.when(t == 0)
     def _():
@@ -598,7 +606,7 @@
             V((4, PEERS, ROWS, 128), bf16), V((PEERS, ROWS, 128), bf16), V((4, ROWS, 128), bf16),
             V((NX, 64, WIDTH), bf16), V((SEQS, GROUPS, GW, STATE), bf16),
             V((2, 8, ROWS, 512), bf16), V((8, ROWS, 640), bf16), V((NX, 32, 128), bf16),
-            pltpu.SMEM((SEQS,), i32), DMA((21,)), DMA((19,)), DMA((19,)),
+            pltpu.SMEM((SEQS,), i32), DMA((21,)), DMA((19,)), DMA((20,)),
             pltpu.SemaphoreType.REGULAR((3, 2)),
         ],
         compiler_params=pltpu.CompilerParams(

time: 38.9 us -> 38.9 us (level)
  no operation moved by 1% of the time
where the time goes in v8:
time: 38.9 us; the launch traced here: 38.8 us
  Pallas kernels  38.2 us (98%)
  between operations  0.65 us (2%)
    pallas_call x1, Pallas kernels, local(): pl.pallas_call(kernel, out_shape=outs, in_specs=[anywhere] * 21, out_spec...  36.9 us
    pallas_call x1, Pallas kernels, local(): pl.pallas_call(finish, out_shape=finals, in_specs=[vmem] * 7, out_specs=[...  1.25 us

profile of v8, /device:TPU:1, one launch (start us, length us, event | category | flops | bytes accessed | tf_op | source)
XLA Modules:
  0.0 38.8 jit_solution(11221492512947586546)
XLA Ops:
  0.6 36.9 %shard_map.252 = (bf16[8,32,128]{2,1,0:T(8,128)(2,1)S(1)}, f32[2,24,64,128]{3,2,1,0:T(8,128)S(1)}, bf16[2,4,1536]{2,1,0:T(4,128)(2,1)S(1)}, bf16[2,4,512]{2,1,0:...) custom-call(bf16[64,4,64]{2,1,0:T(4,128)(2,1)} %tok_h.1, ...), custom_call_target="tpu_custom_call" | custom-call | tf_op jit(solution)/shard_map/pallas_call | solution.py:592
  37.6 1.3 %shard_map.253 = (bf16[64,4,64]{2,1,0:T(4,128)(2,1)}, f32[2,24,64,128]{3,2,1,0:T(8,128)}, bf16[2,4,1536]{2,1,0:T(4,128)(2,1)}, bf16[2,4,512]{2,1,0:T(4,128)(2,1)...) custom-call(bf16[8,32,128]{2,1,0:T(8,128)(2,1)S(1)} %get-tuple-element.21.fr, ...), custom_call_target="tpu_custom_call" | custom-call | tf_op jit(solution)/shard_map/pallas_call | solution.py:624
